TPU v7x, 32 devices: a whole 2x2x4 slice. The times are simulated.
32 devices in a mesh: sp: 8 (over z, x), tp: 4 (over y, core).
Axes of the slice: x: 2, y: 2, z: 4, core: 2. Of those that a mesh axis runs over, the one named last changes fastest.
Arguments:
- residual_layer_input: bfloat16 [2048, 2048], P(('sp', 'tp')), may hold values from -6 to 6
- value_projected: bfloat16 [2048, 4096], P('sp', 'tp'), may hold values from -6 to 6
- key_projected: bfloat16 [2048, 2048], P('sp', 'tp'), may hold values from -6 to 6
- query_projected: bfloat16 [2048, 2048], P('sp', 'tp'), may hold values from -6 to 6
- output_gate_projected: bfloat16 [2048, 4096], P('sp', 'tp'), may hold values from -6 to 6
- step_projected_raw: bfloat16 [2, 2048, 64], P(None, 'sp', 'tp'), may hold values from -5.5 to 5
- head_decay_logarithm: float32 [2, 64], P(None, 'tp'), may hold values from -15 to -2.9
- position_extra_decay: float32 [2048, 64], P('sp', 'tp'), may hold values from -2.1 to 0
- value_filter_weight: bfloat16 [5, 4096], P(None, 'tp'), may hold values from -2.5 to 2.5
- key_filter_weight: bfloat16 [5, 2048], P(None, 'tp'), may hold values from -2.5 to 2.5
- query_filter_weight: bfloat16 [5, 2048], P(None, 'tp'), may hold values from -2.5 to 2.5
- head_norm_gain: float32 [4096], P('tp'), may hold values from 0.1 to 1.9
- mixer_output_matrix: bfloat16 [4096, 2048], P(None, 'tp'), may hold values from -0.09375 to 0.09375
- expert_norm_gain: float32 [2048], replicated, may hold values from 0.1 to 1.9
- routes: int32 [2048, 2], P('sp'), may hold values from 0 to 7, all different within a row; in each aligned block of 64 rows (0 to 63, 64 to 127, ...) at most 32 rows name the same one
- chosen_expert_weight: float32 [2048, 2], P(('sp', 'tp')), may hold values from 0.1 to 1
- expert_gate_matrix: bfloat16 [8, 2048, 4096], P('sp', None, 'tp'), may hold values from -0.125 to 0.125
- expert_up_matrix: bfloat16 [8, 2048, 4096], P('sp', None, 'tp'), may hold values from -0.125 to 0.125
- expert_down_matrix: bfloat16 [8, 4096, 2048], P('sp', 'tp'), may hold values from -0.09375 to 0.09375
Outputs:
- layer_output: bfloat16 [2048, 2048], P(('sp', 'tp'))
Inputs may be any that keep to these rules, and one draw needn't show every extreme that they name: `routes`: each row names 2 different experts; the rows of one device (aligned blocks of 64 rows) name one expert 32 times at most, and that most is reached.
All inputs are finite; a program needn't handle non-finite values.
Results may differ from a plain program's by a relative error of at most 0.015.
Values may be sent and summed in bfloat16 or wider, within the bound.
A program may use at most 64 MiB of HBM per device.

v0:
```python
import functools

import jax
import jax.numpy as jnp
from jax import lax
from jax.experimental import pallas as pl
from jax.experimental.pallas import tpu as pltpu
from jax.sharding import PartitionSpec as P

HEAD_DIM = 64
STATE = 128
BLOCK = 128
TAPS = 5


epsilon = 1e-06
highest = lax.Precision.HIGHEST


MESH = pl.DeviceIdType.MESH


def remote(src, dst, send, recv, device):
    return pltpu.make_async_remote_copy(
        src_ref=src,
        dst_ref=dst,
        send_sem=send,
        recv_sem=recv,
        device_id=device,
        device_id_type=MESH,
    )


def greet(devices):
    barrier = pltpu.get_barrier_semaphore()
    for device in devices:
        pl.semaphore_signal(barrier, inc=1, device_id=device, device_id_type=MESH)
    pl.semaphore_wait(barrier, len(devices))


def vmem(count):
    return [pl.BlockSpec(memory_space=pltpu.VMEM)] * count


def dma(*shape):
    return pltpu.SemaphoreType.DMA(shape)


def params(number):
    return pltpu.CompilerParams(collective_id=number, has_side_effects=True)


def each(count, body):
    lax.fori_loop(0, count, lambda k, _: (body(k), 0)[1], 0)


def exchange_kernel(axis, n, k, *refs):
    ins, outs = refs[:k], refs[k : 2 * k]
    send, recv, local = refs[2 * k :]
    me = lax.axis_index(axis)
    greet([{axis: lax.rem(me + d, n)} for d in range(1, n)])
    copies = []
    for d in range(1, n):
        peer = lax.rem(me + d, n)
        for a in range(k):
            copies.append(
                remote(ins[a].at[peer], outs[a].at[me], send.at[a, d], recv.at[a, d], {axis: peer})
            )
    for a in range(k):
        copies.append(pltpu.make_async_copy(ins[a].at[me], outs[a].at[me], local.at[a]))
    for copy in copies:
        copy.start()
    for copy in copies:
        copy.wait()


def exchange(arrays, axis, number):
    n, k = lax.axis_size(axis), len(arrays)
    return pl.pallas_call(
        functools.partial(exchange_kernel, axis, n, k),
        out_shape=[jax.ShapeDtypeStruct(a.shape, a.dtype) for a in arrays],
        in_specs=vmem(k),
        out_specs=vmem(k),
        scratch_shapes=[dma(k, n), dma(k, n), dma(k)],
        compiler_params=params(number),
    )(*arrays)


def edges_kernel(n, x, out, send, recv):
    me = lax.axis_index("sp")
    left, right = lax.rem(me + n - 1, n), lax.rem(me + 1, n)
    greet([{"sp": left}, {"sp": right}])
    copies = [
        remote(x.at[1], out.at[0], send.at[0], recv.at[0], {"sp": right}),
        remote(x.at[0], out.at[1], send.at[1], recv.at[1], {"sp": left}),
    ]
    for copy in copies:
        copy.start()
    for copy in copies:
        copy.wait()


def edges(x, number):
    return pl.pallas_call(
        functools.partial(edges_kernel, lax.axis_size("sp")),
        out_shape=jax.ShapeDtypeStruct(x.shape, x.dtype),
        in_specs=vmem(1),
        out_specs=vmem(1)[0],
        scratch_shapes=[dma(2), dma(2)],
        compiler_params=params(number),
    )(x)


def tp_places(tp):
    j = lax.axis_index("tp")
    core = lax.rem(j, 2)
    chip = lax.div(j, 2)
    return j, chip, core, tp // 2, chip * 2 + (1 - core)


def gather_kernel(tp, pieces, x, out, send, recv, rsend, rrecv, local):
    j, chip, core, chips, partner = tp_places(tp)
    width = x.shape[1]
    piece = x.shape[0] // pieces
    others = [lax.rem(chip + d, chips) * 2 + core for d in range(1, chips)]
    greet([{"tp": o} for o in others] + [{"tp": partner}])

    def place(b, r):
        return out.at[pl.ds(r * piece, piece), pl.ds(pl.multiple_of(b * width, 128), width)]

    own = pltpu.make_async_copy(
        x, out.at[:, pl.ds(pl.multiple_of(j * width, 128), width)], local.at[0]
    )
    own.start()
    waits = []
    for r in range(pieces):
        part = x.at[pl.ds(r * piece, piece)]
        for d in range(1, chips):
            copy = remote(part, place(j, r), send.at[r, d], recv.at[r, d], {"tp": others[d - 1]})
            copy.start()
            waits.append(copy)
    relays = []
    for r in range(pieces):
        part = x.at[pl.ds(r * piece, piece)]
        copy = remote(part, place(j, r), rsend.at[r, 0], rrecv.at[r, 0], {"tp": partner})
        copy.start()
        relays.append(copy)
    for r in range(pieces):
        for d in range(1, chips):
            came = lax.rem(chip + chips - d, chips) * 2 + core
            spot = place(came, r)
            remote(spot, spot, send.at[r, d], recv.at[r, d], {"tp": partner}).wait_recv()
            copy = remote(spot, spot, rsend.at[r, d], rrecv.at[r, d], {"tp": partner})
            copy.start()
            relays.append(copy)
    for copy in waits:
        copy.wait_send()
    for copy in relays:
        copy.wait()
    own.wait()


def gather_columns(x, number, pieces=2):
    tp = lax.axis_size("tp")
    sems = dma(pieces, tp // 2)
    return pl.pallas_call(
        functools.partial(gather_kernel, tp, pieces),
        out_shape=jax.ShapeDtypeStruct((x.shape[0], x.shape[1] * tp), x.dtype),
        in_specs=vmem(1),
        out_specs=vmem(1)[0],
        scratch_shapes=[sems, sems, sems, sems, dma(1)],
        compiler_params=params(number),
    )(x)


def spread_kernel(sp, tp, ahead, x, out, asend, arecv, fsend, frecv, rsend, rrecv, local):
    me = lax.axis_index("sp")
    j, chip, core, chips, partner = tp_places(tp)
    others = [lax.rem(chip + d, chips) * 2 + core for d in range(1, chips)]
    greet(
        [{"sp": lax.rem(me + d, sp)} for d in range(1, sp)]
        + [{"tp": o} for o in others]
        + [{"tp": partner}]
    )

    def across(d):
        peer = lax.rem(me + d, sp)
        return remote(x.at[peer], out.at[j, me], asend.at[d], arecv.at[d], {"sp": peer})

    def forward(d, k):
        spot = out.at[j, lax.rem(me + sp - d, sp)]
        return remote(spot, spot, fsend.at[d, k], frecv.at[d, k], {"tp": others[k - 1]})

    def relay(d, k):
        came = lax.rem(chip + chips - k, chips) * 2 + core
        spot = out.at[came, lax.rem(me + sp - d, sp)]
        return remote(spot, spot, rsend.at[d, k], rrecv.at[d, k], {"tp": partner})

    own = pltpu.make_async_copy(x.at[me], out.at[j, me], local.at[0])
    own.start()
    each(min(ahead, sp - 1), lambda d: across(d + 1).start())

    def onward(d):
        for k in range(1, chips):
            forward(d, k).start()
        relay(d, 0).start()

    def pass_on(d):
        for k in range(1, chips):
            forward(d, k).wait_recv()
            relay(d, k).start()

    own.wait()
    onward(0)

    def step(d):
        across(d + 1).wait_recv()

        @pl.when(d + 1 + ahead < sp)
        def _():
            across(d + 1 + ahead).start()

        onward(d + 1)
        pass_on(d)

    each(sp - 1, step)
    pass_on(sp - 1)

    def finish(d):
        for k in range(1, chips):
            forward(d, k).wait_send()
        for k in range(chips):
            relay(d, k).wait()

    each(sp, finish)
    each(sp - 1, lambda d: across(d + 1).wait_send())


def spread_rows(x, number):
    sp, tp = lax.axis_size("sp"), lax.axis_size("tp")
    pair = dma(sp, tp // 2)
    return pl.pallas_call(
        functools.partial(spread_kernel, sp, tp, 3),
        out_shape=jax.ShapeDtypeStruct((tp,) + x.shape, x.dtype),
        in_specs=vmem(1),
        out_specs=vmem(1)[0],
        scratch_shapes=[dma(sp), dma(sp), pair, pair, pair, pair, dma(1)],
        compiler_params=params(number),
    )(x)


def collect_kernel(
    sp, tp, x, out, first, joined, second, total, csend, crecv, fsend, frecv, asend, arecv, local
):
    me = lax.axis_index("sp")
    j, chip, core, chips, partner = tp_places(tp)
    others = [lax.rem(chip + d, chips) * 2 + core for d in range(1, chips)]
    greet(
        [{"sp": lax.rem(me + d, sp)} for d in range(1, sp)]
        + [{"tp": o} for o in others]
        + [{"tp": partner}]
    )

    def rows(d):
        return lax.rem(me + d, sp)

    def aim(k):
        return lax.rem(chip + k, chips)

    def beside(d, k):
        s = rows(d)
        return remote(
            x.at[aim(k) * 2 + (1 - core), s],
            first.at[k, s],
            csend.at[d, k],
            crecv.at[d, k],
            {"tp": partner},
        )

    def over(d, k):
        s = rows(d)
        return remote(
            joined.at[k, s], second.at[k, s], fsend.at[d, k], frecv.at[d, k], {"tp": others[k - 1]}
        )

    def back(d):
        s = rows(d)
        return remote(total.at[s], out.at[me], asend.at[d], arecv.at[d], {"sp": s})

    def begin(i):
        d = lax.rem(i + 1, sp)
        for k in range(chips):
            beside(d, lax.rem(k + 1, chips)).start()

    each(sp, begin)

    def join(d):
        s = rows(d)
        for k in range(1, chips):
            beside(d, k).wait_recv()
            mine = x[aim(k) * 2 + core, s].astype(jnp.float32)
            joined[k, s] = (mine + first[k, s].astype(jnp.float32)).astype(joined.dtype)
            over(d, k).start()

    def close(d):
        s = rows(d)
        beside(d, 0).wait_recv()
        value = x[j, s].astype(jnp.float32) + first[0, s].astype(jnp.float32)
        for k in range(1, chips):
            over(d, k).wait_recv()
            value = value + second[k, s].astype(jnp.float32)
        total[s] = value.astype(total.dtype)

    join(lax.rem(1, sp))

    def step(i):
        join(lax.rem(i + 2, sp))
        close(i + 1)
        back(i + 1).start()

    each(sp - 1, step)
    close(0)
    own = pltpu.make_async_copy(total.at[me], out.at[me], local.at[0])
    own.start()

    def finish(d):
        for k in range(chips):
            beside(d, k).wait_send()
        for k in range(1, chips):
            over(d, k).wait_send()

    each(sp, finish)
    each(sp - 1, lambda d: back(d + 1).wait())
    own.wait()


def collect_rows(x, number):
    sp, tp = lax.axis_size("sp"), lax.axis_size("tp")
    chips = tp // 2
    pair = dma(sp, chips)
    buffer = pltpu.VMEM((chips,) + x.shape[1:], x.dtype)
    return pl.pallas_call(
        functools.partial(collect_kernel, sp, tp),
        out_shape=jax.ShapeDtypeStruct(x.shape[1:], x.dtype),
        in_specs=vmem(1),
        out_specs=vmem(1)[0],
        scratch_shapes=[
            buffer,
            buffer,
            buffer,
            pltpu.VMEM(x.shape[1:], x.dtype),
            pair,
            pair,
            pair,
            pair,
            dma(sp),
            dma(sp),
            dma(1),
        ],
        compiler_params=params(number),
    )(x)


def padded_2(cells, width):
    count, here = lax.axis_size("sp"), lax.axis_index("sp")
    came = edges(jnp.stack([cells[:width], cells[-width:]]), 1)
    before = jnp.where(here > 0, came[0], jnp.zeros_like(came[0]))
    after = jnp.where(here < count - 1, came[1], jnp.zeros_like(came[1]))
    return jnp.concatenate([before, cells, after], axis=0)


def carried_states(forward_sum, forward_final, backward_sum, backward_final):
    count = lax.axis_size("sp")
    shape = forward_final.shape
    per_head = shape[-2]
    states = jnp.stack([forward_final, backward_final]).astype(jnp.bfloat16)
    states = states.reshape(2, count, -1, shape[-1]).swapaxes(0, 1)
    totals = jnp.stack([forward_sum, backward_sum]).reshape(2, -1)
    totals = jnp.repeat(totals, per_head, axis=1).reshape(2, count, -1).swapaxes(0, 1)
    states, totals = exchange([states, totals], "sp", 2)
    factors = jnp.exp(totals)[..., None]
    parts = states.astype(jnp.float32)
    forward, backward = [], []
    held = jnp.zeros(parts.shape[2:], jnp.float32)
    for s in range(count):
        forward.append(held)
        held = factors[s, 0] * held + parts[s, 0]
    held = jnp.zeros(parts.shape[2:], jnp.float32)
    for s in reversed(range(count)):
        backward.append(held)
        held = factors[s, 1] * held + parts[s, 1]
    both = jnp.stack([jnp.stack(forward), jnp.stack(backward[::-1])], axis=1)
    (both,) = exchange([both.astype(jnp.bfloat16)], "sp", 3)
    both = both.astype(jnp.float32)
    return both[:, 0].reshape(shape), both[:, 1].reshape(shape)


def prefix_matrix(length):
    row_index = lax.broadcasted_iota(jnp.int32, (length, length), 0)
    column_index = lax.broadcasted_iota(jnp.int32, (length, length), 1)
    return (column_index <= row_index).astype(jnp.float32)


def local_chain(states, totals, reverse):

    def advance(carried, operands):
        block_state, block_total = operands
        return (jnp.exp(block_total)[..., None, None] * carried + block_state, carried)

    start_state = jnp.zeros(states.shape[1:], jnp.float32)
    return lax.scan(advance, start_state, (states, totals), reverse=reverse)


def mix_tokens(
    value_projected,
    key_projected,
    query_projected,
    output_gate_projected,
    step_projected_raw,
    head_decay_logarithm,
    position_extra_decay,
    value_filter_weight,
    key_filter_weight,
    query_filter_weight,
    head_norm_gain,
):
    tokens = value_projected.shape[0]
    value_width = value_projected.shape[1]
    key_width = key_projected.shape[1]
    head_count = step_projected_raw.shape[2]
    group_count = key_width // STATE
    per_group = head_count // group_count
    blocks = tokens // BLOCK
    joined = jnp.concatenate([value_projected, key_projected, query_projected], axis=1)
    padded = padded_2(joined, (TAPS - 1) // 2).astype(jnp.float32)
    weights = jnp.concatenate(
        [value_filter_weight, key_filter_weight, query_filter_weight], axis=1
    ).astype(jnp.float32)
    filtered = weights[0] * padded[0:tokens]
    for offset in range(1, TAPS):
        filtered = filtered + weights[offset] * padded[offset : offset + tokens]
    values = filtered[:, :value_width].astype(jnp.bfloat16)
    key_rows = jax.nn.silu(filtered[:, value_width : value_width + key_width]).astype(jnp.bfloat16)
    key_rows = key_rows.reshape(blocks, BLOCK, group_count, STATE)
    query_rows = jax.nn.silu(filtered[:, value_width + key_width :]).astype(jnp.bfloat16)
    query_rows = query_rows.reshape(blocks, BLOCK, group_count, STATE)
    positive_step_sizes = jax.nn.softplus(step_projected_raw.astype(jnp.float32))
    decay_logarithm = (
        -jnp.exp(head_decay_logarithm)[:, None, :] * positive_step_sizes
        + position_extra_decay[None]
    )
    scaled = (
        values.astype(jnp.float32).reshape(tokens, head_count, HEAD_DIM)[None]
        * positive_step_sizes[..., None]
    ).astype(jnp.bfloat16)
    scaled = scaled.reshape(2, blocks, BLOCK, group_count, per_group, HEAD_DIM)
    log_blocks = decay_logarithm.reshape(2, blocks, BLOCK, group_count, per_group)
    running = jnp.einsum("ls,dbsgh->dblgh", prefix_matrix(BLOCK), log_blocks, precision=highest)
    forward_cum = running[0]
    backward_excl = running[1] - log_blocks[1]
    forward_total = running[0][:, -1]
    backward_total = running[1][:, -1]
    scores = jnp.einsum("blgn,bsgn->blsg", query_rows, key_rows, preferred_element_type=jnp.float32)
    position = lax.broadcasted_iota(jnp.int32, (BLOCK,), 0)
    lower_mask = (position[None, :] <= position[:, None])[None, :, :, None, None]
    upper_mask = (position[None, :] >= position[:, None])[None, :, :, None, None]
    forward_gap = jnp.where(lower_mask, forward_cum[:, :, None] - forward_cum[:, None, :], -jnp.inf)
    backward_gap = jnp.where(
        upper_mask, backward_excl[:, None, :] - backward_excl[:, :, None], -jnp.inf
    )
    forward_weight = (scores[..., None] * jnp.exp(forward_gap)).astype(jnp.bfloat16)
    backward_weight = (scores[..., None] * jnp.exp(backward_gap)).astype(jnp.bfloat16)
    inner = jnp.einsum(
        "blsgh,bsghp->blghp", forward_weight, scaled[0], preferred_element_type=jnp.float32
    )
    inner = inner + jnp.einsum(
        "blsgh,bsghp->blghp", backward_weight, scaled[1], preferred_element_type=jnp.float32
    )
    key_wide = key_rows.astype(jnp.float32)[:, :, :, None, :]
    forward_keys = (jnp.exp(forward_total[:, None] - forward_cum)[..., None] * key_wide).astype(
        jnp.bfloat16
    )
    backward_keys = (jnp.exp(backward_excl)[..., None] * key_wide).astype(jnp.bfloat16)
    forward_state = jnp.einsum(
        "bsghn,bsghp->bghpn", forward_keys, scaled[0], preferred_element_type=jnp.float32
    )
    backward_state = jnp.einsum(
        "bsghn,bsghp->bghpn", backward_keys, scaled[1], preferred_element_type=jnp.float32
    )
    forward_final, forward_before = local_chain(forward_state, forward_total, False)
    backward_final, backward_before = local_chain(backward_state, backward_total, True)
    forward_sum = jnp.sum(forward_total, axis=0)
    backward_sum = jnp.sum(backward_total, axis=0)
    entering, leaving = carried_states(
        forward_sum, forward_final, backward_sum, backward_final
    )
    forward_prior = jnp.cumsum(forward_total, axis=0) - forward_total
    backward_after = backward_sum[None] - jnp.cumsum(backward_total, axis=0)
    forward_in = jnp.exp(forward_prior)[..., None, None] * entering[None] + forward_before
    backward_in = jnp.exp(backward_after)[..., None, None] * leaving[None] + backward_before
    forward_read = jnp.exp(forward_cum)[..., None] * jnp.einsum(
        "blgn,bghpn->blghp",
        query_rows,
        forward_in.astype(jnp.bfloat16),
        preferred_element_type=jnp.float32,
    )
    backward_read = jnp.exp(backward_total[:, None] - backward_excl)[..., None] * jnp.einsum(
        "blgn,bghpn->blghp",
        query_rows,
        backward_in.astype(jnp.bfloat16),
        preferred_element_type=jnp.float32,
    )
    mixer_raw = (inner + forward_read + backward_read).reshape(tokens, head_count, HEAD_DIM)
    gated = mixer_raw * jax.nn.silu(output_gate_projected.astype(jnp.float32)).reshape(
        tokens, head_count, HEAD_DIM
    )
    inverse_rms = lax.rsqrt(jnp.mean(gated * gated, axis=-1, keepdims=True) + epsilon)
    head_normed = (gated * inverse_rms * head_norm_gain.reshape(head_count, HEAD_DIM)).astype(
        jnp.bfloat16
    )
    return head_normed.reshape(tokens, head_count * HEAD_DIM)


def slot_table(route_rows, experts, capacity):
    flat_ids = route_rows.reshape(-1)
    expert_ids = lax.broadcasted_iota(jnp.int32, (flat_ids.shape[0], experts), 1)
    matches = (flat_ids[:, None] == expert_ids).astype(jnp.int32)
    earlier = jnp.cumsum(matches, axis=0) - matches
    rank_in = jnp.sum(matches * earlier, axis=1)
    return (flat_ids * capacity + rank_in).reshape(route_rows.shape)


def dispatch_rows(slots, token_rows, places):
    place_ids = lax.broadcasted_iota(jnp.int32, (places,) + slots.shape, 0)
    one_hot = jnp.sum((place_ids == slots[None]).astype(jnp.float32), axis=2).astype(jnp.bfloat16)
    return jnp.dot(one_hot, token_rows, preferred_element_type=jnp.float32).astype(jnp.bfloat16)


def shards(
    residual_layer_input,
    value_projected,
    key_projected,
    query_projected,
    output_gate_projected,
    step_projected_raw,
    head_decay_logarithm,
    position_extra_decay,
    value_filter_weight,
    key_filter_weight,
    query_filter_weight,
    head_norm_gain,
    mixer_output_matrix,
    expert_norm_gain,
    routes,
    chosen_expert_weight,
    expert_gate_matrix,
    expert_up_matrix,
    expert_down_matrix,
):
    heads_out = mix_tokens(
        value_projected,
        key_projected,
        query_projected,
        output_gate_projected,
        step_projected_raw,
        head_decay_logarithm,
        position_extra_decay,
        value_filter_weight,
        key_filter_weight,
        query_filter_weight,
        head_norm_gain,
    )
    projected = jnp.dot(
        gather_columns(heads_out, 4),
        mixer_output_matrix,
        preferred_element_type=jnp.float32,
    ).astype(jnp.bfloat16)
    tp = lax.axis_size("tp")
    (columns,) = exchange([projected.reshape(tp, -1, projected.shape[1])], "tp", 5)
    mixer_out = columns.swapaxes(0, 1).reshape(columns.shape[1], -1)
    middle = (residual_layer_input.astype(jnp.float32) + mixer_out.astype(jnp.float32)).astype(
        jnp.bfloat16
    )
    residual = middle.astype(jnp.float32)
    normed = (
        residual
        * lax.rsqrt(jnp.mean(residual * residual, axis=-1, keepdims=True) + epsilon)
        * expert_norm_gain
    ).astype(jnp.bfloat16)
    own_rows = normed.shape[0]
    model_width = normed.shape[1]
    top_count = routes.shape[1]
    experts = lax.axis_size("sp")
    capacity = 2 * own_rows * top_count // experts
    places = experts * capacity
    position = lax.axis_index("tp")
    own_routes = lax.dynamic_slice_in_dim(routes, position * own_rows, own_rows, 0)
    own_slots = slot_table(own_routes, experts, capacity)
    outgoing = dispatch_rows(own_slots, normed, places)
    arrived = spread_rows(outgoing.reshape(experts, capacity, model_width), 6)
    slot_rows = arrived.reshape(-1, model_width)
    gate_value = jnp.dot(slot_rows, expert_gate_matrix[0], preferred_element_type=jnp.float32)
    up_value = jnp.dot(slot_rows, expert_up_matrix[0], preferred_element_type=jnp.float32)
    hidden = (jax.nn.silu(gate_value) * up_value).astype(jnp.bfloat16)
    partial_sum = jnp.dot(hidden, expert_down_matrix[0], preferred_element_type=jnp.float32).astype(
        jnp.bfloat16
    )
    returned = collect_rows(partial_sum.reshape(arrived.shape), 7)
    chosen = (
        lax.broadcasted_iota(jnp.int32, (own_rows, top_count, places), 2) == own_slots[:, :, None]
    )
    mixing = jnp.sum(jnp.where(chosen, chosen_expert_weight[:, :, None], 0.0), axis=1)
    expert_mix = jnp.dot(
        mixing, returned.reshape(places, model_width).astype(jnp.float32), precision=highest
    )
    return (residual + expert_mix).astype(jnp.bfloat16)


def solution(mesh):
    return jax.shard_map(
        shards,
        mesh=mesh,
        in_specs=(
            P(("sp", "tp"), None),
            P("sp", "tp"),
            P("sp", "tp"),
            P("sp", "tp"),
            P("sp", "tp"),
            P(None, "sp", "tp"),
            P(None, "tp"),
            P("sp", "tp"),
            P(None, "tp"),
            P(None, "tp"),
            P(None, "tp"),
            P("tp"),
            P(None, "tp"),
            P(),
            P("sp", None),
            P(("sp", "tp"), None),
            P("sp", None, "tp"),
            P("sp", None, "tp"),
            P("sp", "tp", None),
        ),
        out_specs=P(("sp", "tp"), None),
        check_vma=False,
    )
```

profile of v0, /device:TPU:0, one launch (start us, length us, event | category | flops | bytes accessed | tf_op | source)
XLA Modules:
  0.0 224.7 jit_solution(2686266825265112798)
XLA Ops:
  0.0 1.1 constant_dynamic-update-slice_fusion.2
  1.1 1.0 constant_dynamic-update-slice_fusion.1
  2.1 1.0 constant_dynamic-update-slice_fusion
  3.1 0.6 pad_maximum_fusion.1.x
  3.8 9.5 %shard_map.181 = bf16[2,2,2048]{2,1,0:T(2,128)(2,1)} custom-call(bf16[2,2,2048]{2,1,0:T(2,128)(2,1)} %pad_maximum_fusion.1.x), custom_call_target="tpu_custom_call" | custom-call | tf_op jit(solution)/shard_map/pallas_call | solution.py:104
  13.3 0.7 fusion.88
  14.0 0.3 maximum_convert_fusion
  14.4 1.2 fusion.12
  15.6 1.0 fusion.46
  16.7 1.6 copy.105
  18.3 0.2 multiply_convert_fusion.5
  18.6 0.9 fusion.102
  19.5 0.1 squeeze.105
  19.6 1.0 multiply_convert_fusion.12
  20.7 0.2 convolution_bitcast_fusion.3
  20.9 0.2 slice_reduce_fusion
  21.3 1.3 fusion.28
  22.7 0.4 while.31
  22.8 0.1 bitcast_add_fusion.5
  23.0 0.1 bitcast_add_fusion.5
  23.1 0.8 convert.66
  24.0 1.2 squeeze.104
  25.2 1.1 fusion.27
  26.4 0.4 while.30
  26.9 0.5 copy-done.7
  27.3 0.9 maximum_bitcast_fusion.refs_0_
  28.5 0.6 copy.167
  29.1 13.7 %shard_map.182 = (bf16[8,2,128,128]{3,2,1,0:T(8,128)(2,1)}, f32[8,2,128]{2,1,0:T(2,128)}) custom-call(bf16[8,2,128,128]{3,2,1,0:T(8,128)(2,1)} %maximum_bitcast_fusion.refs_0_, f32[8,2,128]{2,1,0:T(2,128)} %bitcast.292), custom_call_target="tpu_custom_call" | custom-call | tf_op jit(solution)/shard_map/pallas_call | solution.py:79
  42.8 1.1 convert_element_type.120
  44.0 0.7 exponential_bitcast_fusion.2
  45.4 0.2 constant_dynamic-update-slice_fusion.18
  46.0 0.9 pad_maximum_fusion.refs_0_
  46.8 17.5 %shard_map.183 = bf16[8,2,128,128]{3,2,1,0:T(8,128)(2,1)} custom-call(bf16[8,2,128,128]{3,2,1,0:T(8,128)(2,1)} %pad_maximum_fusion.refs_0_), custom_call_target="tpu_custom_call" | custom-call | tf_op jit(solution)/shard_map/pallas_call | solution.py:79
  64.3 1.9 fusion.103
  66.3 0.3 convolution_bitcast_fusion.2
  66.6 0.2 copy.108
  66.9 2.1 fusion.26
  69.0 0.9 fusion.20
  69.9 1.4 fusion.19
  71.3 0.3 convert_multiply_fusion
  71.6 1.4 reshape.2013
  73.0 1.8 copy.123
  74.8 3.2 %multiply_reduce_fusion = (f32[2,128,4,4]{1,3,2,0:T(4,128)S(1)}, f32[2,128,4,4,64]{1,4,3,2,0:T(8,128)}) fusion(f32[2,128,4,4,64]{1,4,3,2,0:T(8,128)} %copy.123, f32[2,128,4,4,64]{1,4,3,2,0:T(8,128)S(1)} %copy-done.1, bf16[2,128,4,128,1]{3,2,1,0,4:T(4,128)(2,1)S(1)} %bitcast.279, f32[2,4,4,64,128]{4,3,2,1,0:T(8,128)} %copy-done.2, ...), kind=kOutput, calls=%fused_computation.57 | convolution fusion | flops 69201920 | bytes 5013632 | tf_op jit(solution)/shard_map/blgn,bghpn->blghp/dot_general | solution.py:507
  77.9 2.3 %copy.136 = f32[2,128,4,4,64]{4,3,2,1,0:T(4,128)S(1)} copy(f32[2,128,4,4,64]{1,4,3,2,0:T(8,128)} %get-tuple-element.258) | data formatting | bytes 2097152 | tf_op jit(solution)/shard_map/reshape | solution.py:513
  80.2 1.5 reshape.2012
  81.8 0.3 copy.125
  82.2 0.2 copy-done.16
  82.4 2.2 multiply_convert_fusion.10.x
  84.6 17.9 %shard_map.184 = bf16[256,4096]{1,0:T(8,128)(2,1)} custom-call(bf16[256,1024]{1,0:T(8,128)(2,1)} %multiply_convert_fusion.10.x), custom_call_target="tpu_custom_call" | custom-call | tf_op jit(solution)/shard_map/pallas_call | solution.py:166
  102.5 4.8 %convolution_convert_fusion.1 = bf16[256,512]{1,0:T(8,128)(2,1)} fusion(bf16[256,4096]{1,0:T(8,128)(2,1)} %shard_map.184, bf16[4096,512]{1,0:T(8,128)(2,1)} %param.35), kind=kOutput, calls=%fused_computation.42 | convolution fusion | flops 1073872896 | bytes 6553600 | tf_op jit(solution)/shard_map/dot_general | solution.py:573
  107.3 6.7 %shard_map.185 = bf16[4,64,512]{2,1,0:T(8,128)(2,1)} custom-call(bf16[4,64,512]{2,1,0:T(8,128)(2,1)} %bitcast.289), custom_call_target="tpu_custom_call" | custom-call | tf_op jit(solution)/shard_map/pallas_call | solution.py:79
  114.0 1.0 convert_bitcast_fusion
  115.1 0.2 fusion.43
  115.5 0.1 eq.26
  115.7 0.2 reduce_window_sum.33
  115.9 0.2 select_reduce_fusion.1
  116.1 0.1 reduce_sum.69
  116.5 1.5 convolution_convert_fusion
  117.9 41.8 %shard_map.186 = bf16[4,8,32,2048]{3,2,1,0:T(8,128)(2,1)} custom-call(bf16[8,32,2048]{2,1,0:T(8,128)(2,1)} %bitcast.277), custom_call_target="tpu_custom_call" | custom-call | tf_op jit(solution)/shard_map/pallas_call | solution.py:242
  159.8 8.0 %fusion.2 = f32[1024,1024]{1,0:T(8,128)S(1)} fusion(bf16[1024,2048]{1,0:T(8,128)(2,1)} %bitcast.273, bf16[1,2048,1024]{2,1,0:T(8,128)(2,1)} %param.40), kind=kOutput, calls=%fused_computation.8 | convolution fusion | flops 4294967296 | bytes 12582912 | tf_op jit(solution)/shard_map/dot_general | solution.py:603
  167.8 5.4 %multiply_convert_fusion = bf16[1024,1024]{1,0:T(8,128)(2,1)S(1)} fusion(f32[1024,1024]{1,0:T(8,128)S(1)} %fusion.2, bf16[1024,2048]{1,0:T(8,128)(2,1)S(1)} %bitcast.274, bf16[1,2048,1024]{2,1,0:T(8,128)(2,1)S(1)} %copy-done.20), kind=kOutput, calls=%fused_computation.12 | convolution fusion | flops 4301258752 | bytes 14680064 | tf_op jit(solution)/shard_map/dot_general | solution.py:602
  173.2 6.1 %fusion.6 = bf16[1024,2048]{1,0:T(8,128)(2,1)} fusion(bf16[1024,1024]{1,0:T(8,128)(2,1)S(1)} %multiply_convert_fusion, bf16[1,1024,2048]{2,1,0:T(8,128)(2,1)S(1)} %copy-done.21), kind=kOutput, calls=%fused_computation.13 | convolution fusion | flops 4297064448 | bytes 10485760 | tf_op jit(solution)/shard_map/dot_general | solution.py:605
  179.3 42.7 %shard_map.187 = bf16[8,32,2048]{2,1,0:T(8,128)(2,1)} custom-call(bf16[4,8,32,2048]{3,2,1,0:T(8,128)(2,1)} %bitcast.275), custom_call_target="tpu_custom_call" | custom-call | tf_op jit(solution)/shard_map/pallas_call | solution.py:342
  222.1 2.6 %fusion.11 = bf16[64,2048]{1,0:T(8,128)(2,1)} fusion(f32[64,256]{1,0:T(8,128)S(1)} %select_reduce_fusion, bf16[256,2048]{1,0:T(8,128)(2,1)} %bitcast.276, bf16[64,2048]{1,0:T(8,128)(2,1)S(1)} %get-tuple-element.206), kind=kOutput, calls=%fused_computation.16 | convolution fusion | flops 403046400 | bytes 1638400 | tf_op jit(solution)/shard_map/dot_general | solution.py:613
  (107 shorter events, 3.4 us)
Async XLA Ops:
  1.1 13.3 %copy-start.12 = (bf16[5,1024]{1,0:T(8,128)(2,1)S(1)}, bf16[5,1024]{1,0:T(8,128)(2,1)}, u32[]{:S(2)}) copy-start(bf16[5,1024]{1,0:T(8,128)(2,1)} %param.31) | copy-start | bytes 30724
  1.1 13.3 %copy-start.14 = (bf16[5,512]{1,0:T(8,128)(2,1)S(1)}, bf16[5,512]{1,0:T(8,128)(2,1)}, u32[]{:S(2)}) copy-start(bf16[5,512]{1,0:T(8,128)(2,1)} %param.33) | copy-start | bytes 15364
  1.1 13.3 %copy-start.15 = (bf16[5,512]{1,0:T(8,128)(2,1)S(1)}, bf16[5,512]{1,0:T(8,128)(2,1)}, u32[]{:S(2)}) copy-start(bf16[5,512]{1,0:T(8,128)(2,1)} %param.32) | copy-start | bytes 15364
  15.6 2.6 %copy-start.19 = (f32[2,16]{1,0:T(2,128)S(1)}, f32[2,16]{1,0:T(2,128)}, u32[]{:S(2)}) copy-start(f32[2,16]{1,0:T(2,128)} %param.29) | copy-start | bytes 388
  15.6 2.7 %copy-start.10 = (bf16[2,256,16]{1,2,0:T(8,128)(2,1)S(1)}, bf16[2,256,16]{1,2,0:T(8,128)(2,1)}, u32[]{:S(2)}) copy-start(bf16[2,256,16]{1,2,0:T(8,128)(2,1)} %param.28) | copy-start | bytes 49156
  15.6 2.7 %copy-start.11 = (f32[256,16]{0,1:T(8,128)S(1)}, f32[256,16]{0,1:T(8,128)}, u32[]{:S(2)}) copy-start(f32[256,16]{0,1:T(8,128)} %param.30) | copy-start | bytes 49156
  19.6 2.9 %copy-start.4 = (bf16[2,128,4,4,64]{1,0,4,3,2:T(2,128)(2,1)}, bf16[2,128,4,4,64]{1,0,4,3,2:T(2,128)(2,1)S(1)}, u32[]{:S(2)}) copy-start(bf16[2,128,4,4,64]{1,0,4,3,2:T(2,128)(2,1)S(1)} %squeeze.105) | copy-start | bytes 1572868
  23.1 2.0 copy-start.2
  25.1 1.1 copy-start.6
  26.4 1.0 copy-start.7
  46.0 20.3 %copy-start.8 = (bf16[256,512]{1,0:T(8,128)(2,1)S(1)}, bf16[256,512]{1,0:T(8,128)(2,1)}, u32[]{:S(2)}) copy-start(bf16[256,512]{1,0:T(8,128)(2,1)} %get-tuple-element.220) | copy-start | bytes 786436
  66.6 2.3 %copy-start.5 = (bf16[2,128,4,4,64]{1,0,4,3,2:T(2,128)(2,1)S(1)}, bf16[2,128,4,4,64]{1,0,4,3,2:T(2,128)(2,1)}, u32[]{:S(2)}) copy-start(bf16[2,128,4,4,64]{1,0,4,3,2:T(2,128)(2,1)} %copy-done.4) | copy-start | bytes 1572868
  69.9 1.4 copy-start.3
  73.0 1.8 copy-start.1
  81.7 0.7 copy-start.16
  107.3 7.8 %copy-start.9 = (bf16[64,2048]{1,0:T(8,128)(2,1)S(1)}, bf16[64,2048]{1,0:T(8,128)(2,1)}, u32[]{:S(2)}) copy-start(bf16[64,2048]{1,0:T(8,128)(2,1)} %param.23) | copy-start | bytes 786436
  107.3 8.0 %copy-start.17 = (s32[256,2]{0,1:T(2,128)S(1)}, s32[256,2]{0,1:T(2,128)}, u32[]{:S(2)}) copy-start(s32[256,2]{0,1:T(2,128)} %param.37) | copy-start | bytes 6148
  107.3 9.2 %copy-start.13 = (f32[2048]{0:T(1024)S(1)}, f32[2048]{0:T(1024)}, u32[]{:S(2)}) copy-start(f32[2048]{0:T(1024)} %param.36) | copy-start | bytes 24580
  159.7 8.1 %copy-start = (bf16[4,8,32,2048]{3,2,1,0:T(8,128)(2,1)S(1)}, bf16[4,8,32,2048]{3,2,1,0:T(8,128)(2,1)}, u32[]{:S(2)}) copy-start(bf16[4,8,32,2048]{3,2,1,0:T(8,128)(2,1)} %shard_map.186) | copy-start | bytes 12582916
  159.7 8.1 %copy-start.20 = (bf16[1,2048,1024]{2,1,0:T(8,128)(2,1)S(1)}, bf16[1,2048,1024]{2,1,0:T(8,128)(2,1)}, u32[]{:S(2)}) copy-start(bf16[1,2048,1024]{2,1,0:T(8,128)(2,1)} %param.39) | copy-start | bytes 12582916
  167.8 5.4 %copy-start.21 = (bf16[1,1024,2048]{2,1,0:T(8,128)(2,1)S(1)}, bf16[1,1024,2048]{2,1,0:T(8,128)(2,1)}, u32[]{:S(2)}) copy-start(bf16[1,1024,2048]{2,1,0:T(8,128)(2,1)} %param.41) | copy-start | bytes 12582916
  179.3 42.7 %copy-start.18 = (f32[64,2]{0,1:T(2,128)S(1)}, f32[64,2]{0,1:T(2,128)}, u32[]{:S(2)}) copy-start(f32[64,2]{0,1:T(2,128)} %param.38) | copy-start | bytes 1540
where the time goes:
time: 226 us; the launch traced here: 225 us
  Pallas kernels  150 us (66%)
  matrix products  38.6 us (17%)
  local copies, waits for them, and re-layouts  19.7 us (9%)
  other arithmetic  15.5 us (7%)
    pallas_call x1, Pallas kernels, collect_rows(): pl.pallas_call(functools.partial(collect_kernel, sp, tp), out_shape=jax.S...  42.7 us
    pallas_call x1, Pallas kernels, spread_rows(): pl.pallas_call(functools.partial(spread_kernel, sp, tp, 3), out_shape=jax...  41.8 us
    pallas_call x3, Pallas kernels, exchange(): pl.pallas_call(functools.partial(exchange_kernel, axis, n, k), out_shape=...  37.9 us
    pallas_call x1, Pallas kernels, gather_columns(): pl.pallas_call(functools.partial(gather_kernel, tp, pieces), out_shape=ja...  17.9 us
    pallas_call x1, Pallas kernels, edges(): pl.pallas_call(functools.partial(edges_kernel, lax.axis_size('sp')), out_...  9.52 us
    dot_general x1, matrix products, shards(): jnp.dot(slot_rows, expert_up_matrix[0], preferred_element_type=jnp.float32)  8.04 us
    dot_general x1, matrix products, shards(): jnp.dot(hidden, expert_down_matrix[0], preferred_element_type=jnp.float32)  6.06 us
    dot_general x1, matrix products, shards(): jnp.dot(slot_rows, expert_gate_matrix[0], preferred_element_type=jnp.floa...  5.35 us

commit v1 on v0

--- a/solution.py
+++ b/solution.py
@@ -359,6 +359,220 @@
         ],
         compiler_params=params(number),
     )(x)
+
+
+def flip(me, d):
+    out, bit = me, 1
+    while bit <= d:
+        if d & bit:
+            out = out + bit * (1 - 2 * lax.rem(lax.div(out, bit), 2))
+        bit *= 2
+    return out
+
+
+def expert_kernel(
+    sp, tp, x, wgate, wup, wdown, out,
+    arr, part, hidden, first, joined, second, total, vgate, vup, vdown,
+    asend, arecv, fsend, frecv, rsend, rrecv, csend, crecv, osend, orecv, bsend, brecv, local, load,
+):
+    me = lax.axis_index("sp")
+    j, chip, core, chips, partner = tp_places(tp)
+    others = [lax.rem(chip + d, chips) * 2 + core for d in range(1, chips)]
+    cap, width = x.shape[1], x.shape[2]
+    ff = vgate.shape[1]
+    rows = 2 * tp * cap
+    loads = [
+        pltpu.make_async_copy(wgate.at[0], vgate, load.at[0]),
+        pltpu.make_async_copy(wup.at[0], vup, load.at[1]),
+        pltpu.make_async_copy(wdown.at[0], vdown, load.at[2]),
+    ]
+    for copy in loads:
+        copy.start()
+    own = pltpu.make_async_copy(x.at[me], arr.at[me, j], local.at[0])
+    own.start()
+    greet(
+        [{"sp": flip(me, d)} for d in range(1, sp)]
+        + [{"tp": o} for o in others]
+        + [{"tp": partner}]
+    )
+
+    def across(d):
+        peer = flip(me, d)
+        return remote(x.at[peer], arr.at[me, j], asend.at[d], arecv.at[d], {"sp": peer})
+
+    def forward(d, k):
+        spot = arr.at[flip(me, d), j]
+        return remote(spot, spot, fsend.at[d, k], frecv.at[d, k], {"tp": others[k - 1]})
+
+    def relay(d, k):
+        came = lax.rem(chip + chips - k, chips) * 2 + core
+        spot = arr.at[flip(me, d), came]
+        return remote(spot, spot, rsend.at[d, k], rrecv.at[d, k], {"tp": partner})
+
+    def onward(d):
+        if d == 0:
+            own.wait()
+        else:
+            across(d).wait_recv()
+        for k in range(1, chips):
+            forward(d, k).start()
+        relay(d, 0).start()
+
+    def pass_on(d):
+        for k in range(1, chips):
+            forward(d, k).wait_recv()
+            relay(d, k).start()
+
+    def aim(k):
+        return lax.rem(chip + k, chips)
+
+    def beside(d, k):
+        s = flip(me, d)
+        return remote(
+            part.at[s, aim(k) * 2 + (1 - core)],
+            first.at[s, k],
+            csend.at[d, k],
+            crecv.at[d, k],
+            {"tp": partner},
+        )
+
+    def over(d, k):
+        s = flip(me, d)
+        return remote(
+            joined.at[s, k], second.at[s, k], osend.at[d, k], orecv.at[d, k], {"tp": others[k - 1]}
+        )
+
+    def back(d):
+        s = flip(me, d)
+        return remote(total.at[s], out.at[me], bsend.at[d], brecv.at[d], {"sp": s})
+
+    def begin(d):
+        for k in range(chips):
+            beside(d, (k + 1) % chips).start()
+
+    def join(d):
+        s = flip(me, d)
+        for k in range(1, chips):
+            beside(d, k).wait_recv()
+            mine = part[s, aim(k) * 2 + core].astype(jnp.float32)
+            joined[s, k] = (mine + first[s, k].astype(jnp.float32)).astype(joined.dtype)
+            over(d, k).start()
+
+    def close(d):
+        s = flip(me, d)
+        beside(d, 0).wait_recv()
+        value = part[s, j].astype(jnp.float32) + first[s, 0].astype(jnp.float32)
+        for k in range(1, chips):
+            over(d, k).wait_recv()
+            value = value + second[s, k].astype(jnp.float32)
+        if d == 0:
+            out[me] = value.astype(out.dtype)
+        else:
+            total[s] = value.astype(total.dtype)
+            back(d).start()
+
+    tile = min(ff, 256)
+    wide = min(width, 256)
+
+    def gate_up(g):
+        base = flip(me, 2 * g) - lax.rem(flip(me, 2 * g), 2)
+
+        def step(f):
+            cols = pl.ds(pl.multiple_of(f * tile, tile), tile)
+            held = arr[pl.ds(base, 2)].reshape(rows, width)
+            gate = jnp.dot(held, vgate[:, cols], preferred_element_type=jnp.float32)
+            up = jnp.dot(held, vup[:, cols], preferred_element_type=jnp.float32)
+            hidden[:, cols] = (gate / (1.0 + jnp.exp(-gate)) * up).astype(hidden.dtype)
+
+        each(ff // tile, step)
+
+    def down(g):
+        base = flip(me, 2 * g) - lax.rem(flip(me, 2 * g), 2)
+
+        def step(f):
+            cols = pl.ds(pl.multiple_of(f * wide, wide), wide)
+            value = jnp.dot(hidden[...], vdown[:, cols], preferred_element_type=jnp.float32)
+            part[pl.ds(base, 2), :, :, cols] = value.astype(part.dtype).reshape(2, tp, cap, wide)
+
+        each(width // wide, step)
+
+    for d in range(1, sp):
+        across(d).start()
+    ahead = min(4, sp)
+    onward(0)
+    onward(1)
+    onward(2)
+    pass_on(0)
+    onward(3)
+    pass_on(1)
+    for copy in loads[:2]:
+        copy.wait()
+    for g in range(sp // 2):
+        for d in (2 * g, 2 * g + 1):
+            if g > 0:
+                pass_on(d)
+        for d in (2 * g, 2 * g + 1):
+            for k in range(chips):
+                relay(d, k).wait_recv()
+        gate_up(g)
+        for d in (2 * g + ahead, 2 * g + ahead + 1):
+            if d < sp:
+                onward(d)
+        if g == 0:
+            loads[2].wait()
+        down(g)
+        begin(2 * g)
+        begin(2 * g + 1)
+        if g > 0:
+            close(2 * g - 2)
+            close(2 * g - 1)
+        join(2 * g)
+        join(2 * g + 1)
+    close(sp - 2)
+    close(sp - 1)
+    for d in range(sp):
+        for k in range(1, chips):
+            forward(d, k).wait_send()
+            over(d, k).wait_send()
+        for k in range(chips):
+            relay(d, k).wait_send()
+            beside(d, k).wait_send()
+        if d > 0:
+            across(d).wait_send()
+            back(d).wait()
+
+
+def run_experts(x, wgate, wup, wdown, number):
+    sp, tp = lax.axis_size("sp"), lax.axis_size("tp")
+    chips = tp // 2
+    cap, width = x.shape[1:]
+    ff = wgate.shape[2]
+    kind = x.dtype
+    pair = dma(sp, chips)
+    line = dma(sp)
+    piece = pltpu.VMEM((sp, chips, cap, width), kind)
+    return pl.pallas_call(
+        functools.partial(expert_kernel, sp, tp),
+        out_shape=jax.ShapeDtypeStruct(x.shape, kind),
+        in_specs=vmem(1) + [pl.BlockSpec(memory_space=pl.ANY)] * 3,
+        out_specs=vmem(1)[0],
+        scratch_shapes=[
+            pltpu.VMEM((sp, tp, cap, width), kind),
+            pltpu.VMEM((sp, tp, cap, width), kind),
+            pltpu.VMEM((2 * tp * cap, ff), kind),
+            piece,
+            piece,
+            piece,
+            pltpu.VMEM((sp, cap, width), kind),
+            pltpu.VMEM(wgate.shape[1:], kind),
+            pltpu.VMEM(wup.shape[1:], kind),
+            pltpu.VMEM(wdown.shape[1:], kind),
+            line, line, pair, pair, pair, pair, pair, pair, pair, pair, line, line, dma(1), dma(3),
+        ],
+        compiler_params=pltpu.CompilerParams(
+            collective_id=number, has_side_effects=True, vmem_limit_bytes=56 * 2**20
+        ),
+    )(x, wgate, wup, wdown)
 
 
 def padded_2(cells, width):
@@ -597,15 +811,21 @@
     own_routes = lax.dynamic_slice_in_dim(routes, position * own_rows, own_rows, 0)
     own_slots = slot_table(own_routes, experts, capacity)
     outgoing = dispatch_rows(own_slots, normed, places)
-    arrived = spread_rows(outgoing.reshape(experts, capacity, model_width), 6)
-    slot_rows = arrived.reshape(-1, model_width)
-    gate_value = jnp.dot(slot_rows, expert_gate_matrix[0], preferred_element_type=jnp.float32)
-    up_value = jnp.dot(slot_rows, expert_up_matrix[0], preferred_element_type=jnp.float32)
-    hidden = (jax.nn.silu(gate_value) * up_value).astype(jnp.bfloat16)
-    partial_sum = jnp.dot(hidden, expert_down_matrix[0], preferred_element_type=jnp.float32).astype(
-        jnp.bfloat16
-    )
-    returned = collect_rows(partial_sum.reshape(arrived.shape), 7)
+    slotted = outgoing.reshape(experts, capacity, model_width)
+    if capacity % 16 == 0 and experts & (experts - 1) == 0 and experts >= 4:
+        returned = run_experts(
+            slotted, expert_gate_matrix, expert_up_matrix, expert_down_matrix, 6
+        )
+    else:
+        arrived = spread_rows(slotted, 6)
+        slot_rows = arrived.reshape(-1, model_width)
+        gate_value = jnp.dot(slot_rows, expert_gate_matrix[0], preferred_element_type=jnp.float32)
+        up_value = jnp.dot(slot_rows, expert_up_matrix[0], preferred_element_type=jnp.float32)
+        hidden = (jax.nn.silu(gate_value) * up_value).astype(jnp.bfloat16)
+        partial_sum = jnp.dot(hidden, expert_down_matrix[0], preferred_element_type=jnp.float32).astype(
+            jnp.bfloat16
+        )
+        returned = collect_rows(partial_sum.reshape(arrived.shape), 7)
     chosen = (
         lax.broadcasted_iota(jnp.int32, (own_rows, top_count, places), 2) == own_slots[:, :, None]
     )

time: 226 us -> 198 us (0.88)
  matrix products: 38.6 us -> 19.1 us
  Pallas kernels: 150 us -> 139 us
    dot_general x3 -> x0, matrix products: 19.5 us -> none  [the longest x1 8.04 us: shards(): jnp.dot(slot_rows, expert_up_matrix[0], preferred_element_type=jnp.float32)]
    pallas_call x2 -> x1, Pallas kernels: 84.4 us -> 74 us  [run_experts(): pl.pallas_call(functools.partial(expert_kernel, sp, tp), out_shape=jax.Sh...]
where the time goes in v1:
time: 198 us; the launch traced here: 195 us
  Pallas kernels  139 us (70%)
  local copies, waits for them, and re-layouts  19.7 us (10%)
  matrix products  19.1 us (10%)
  other arithmetic  15.5 us (8%)
    pallas_call x1, Pallas kernels, run_experts(): pl.pallas_call(functools.partial(expert_kernel, sp, tp), out_shape=jax.Sh...  74 us
    pallas_call x3, Pallas kernels, exchange(): pl.pallas_call(functools.partial(exchange_kernel, axis, n, k), out_shape=...  37.9 us
    pallas_call x1, Pallas kernels, gather_columns(): pl.pallas_call(functools.partial(gather_kernel, tp, pieces), out_shape=ja...  17.8 us
    pallas_call x1, Pallas kernels, edges(): pl.pallas_call(functools.partial(edges_kernel, lax.axis_size('sp')), out_...  9.52 us
    dot_general x1, matrix products, shards(): jnp.dot(gather_columns(heads_out, 4), mixer_output_matrix, preferred_elem...  4.77 us

profile of v1, /device:TPU:0, one launch (start us, length us, event | category | flops | bytes accessed | tf_op | source)
XLA Modules:
  0.0 194.5 jit_solution(14459066223523517762)
XLA Ops:
  0.0 1.1 constant_dynamic-update-slice_fusion.2
  1.1 1.0 constant_dynamic-update-slice_fusion.1
  2.1 1.0 constant_dynamic-update-slice_fusion
  3.1 0.6 pad_maximum_fusion.1.x
  3.8 9.5 %shard_map.181 = bf16[2,2,2048]{2,1,0:T(2,128)(2,1)} custom-call(bf16[2,2,2048]{2,1,0:T(2,128)(2,1)} %pad_maximum_fusion.1.x), custom_call_target="tpu_custom_call" | custom-call | tf_op jit(solution)/shard_map/pallas_call | solution.py:104
  13.3 0.7 fusion.77
  14.0 0.3 maximum_convert_fusion
  14.4 1.2 fusion.1
  15.6 1.0 fusion.35
  16.6 1.6 copy.105
  18.3 0.2 multiply_convert_fusion.4
  18.6 0.9 fusion.91
  19.4 0.1 squeeze.96
  19.6 1.0 multiply_convert_fusion.11
  20.7 0.2 convolution_bitcast_fusion.3
  20.9 0.2 slice_reduce_fusion
  21.3 1.3 fusion.17
  22.7 0.4 while.31
  22.7 0.1 bitcast_add_fusion.5
  23.0 0.1 bitcast_add_fusion.5
  23.1 0.8 convert.66
  23.9 1.2 squeeze.95
  25.1 1.1 fusion.16
  26.4 0.4 while.30
  26.4 0.1 bitcast_add_fusion.4
  26.7 0.1 bitcast_add_fusion.4
  26.8 0.5 copy-done.6
  27.3 0.8 maximum_bitcast_fusion.refs_0_
  28.5 0.6 copy.167
  29.1 13.7 %shard_map.182 = (bf16[8,2,128,128]{3,2,1,0:T(8,128)(2,1)}, f32[8,2,128]{2,1,0:T(2,128)}) custom-call(bf16[8,2,128,128]{3,2,1,0:T(8,128)(2,1)} %maximum_bitcast_fusion.refs_0_, f32[8,2,128]{2,1,0:T(2,128)} %bitcast.271), custom_call_target="tpu_custom_call" | custom-call | tf_op jit(solution)/shard_map/pallas_call | solution.py:79
  42.8 1.1 convert_element_type.114
  44.0 0.7 exponential_bitcast_fusion.2
  45.0 0.1 constant_dynamic-update-slice_fusion.6
  45.2 0.1 constant_dynamic-update-slice_fusion.4
  45.3 0.2 constant_dynamic-update-slice_fusion.18
  46.0 0.9 pad_maximum_fusion.refs_0_
  46.8 17.5 %shard_map.183 = bf16[8,2,128,128]{3,2,1,0:T(8,128)(2,1)} custom-call(bf16[8,2,128,128]{3,2,1,0:T(8,128)(2,1)} %pad_maximum_fusion.refs_0_), custom_call_target="tpu_custom_call" | custom-call | tf_op jit(solution)/shard_map/pallas_call | solution.py:79
  64.3 1.9 fusion.92
  66.3 0.3 convolution_bitcast_fusion.2
  66.6 0.2 copy.108
  66.8 2.1 %fusion.15 = f32[2,4,4,64,128]{4,3,2,1,0:T(8,128)S(1)} fusion(f32[2,128,4,4]{1,3,2,0:T(4,128)S(1)} %get-tuple-element.233, f32[2,128,128,4]{2,1,3,0:T(8,128)S(1)} %copy.108, pred[128,128]{1,0:T(8,128)(4,1)S(1)} %iota_compare_fusion.4, bf16[2,128,4,4,64]{1,0,4,3,2:T(2,128)(2,1)} %copy-done.5), kind=kOutput, calls=%fused_computation.44 | convolution fusion | flops 69206016 | bytes 2129920 | tf_op jit(solution)/shard_map/blsgh,bsghp->blghp/dot_general | solution.py:687
  68.9 0.9 fusion.9
  69.9 1.4 fusion.8
  71.3 0.3 convert_multiply_fusion
  71.6 1.4 reshape.2005
  73.0 1.7 copy.123
  74.7 3.2 %multiply_reduce_fusion = (f32[2,128,4,4]{1,3,2,0:T(4,128)S(1)}, f32[2,128,4,4,64]{1,4,3,2,0:T(8,128)}) fusion(f32[2,128,4,4,64]{1,4,3,2,0:T(8,128)} %copy.123, f32[2,128,4,4,64]{1,4,3,2,0:T(8,128)S(1)} %copy-done, bf16[2,128,4,128,1]{3,2,1,0,4:T(4,128)(2,1)S(1)} %bitcast.258, f32[2,4,4,64,128]{4,3,2,1,0:T(8,128)} %copy-done.1, ...), kind=kOutput, calls=%fused_computation.49 | convolution fusion | flops 69201920 | bytes 5013632 | tf_op jit(solution)/shard_map/blgn,bghpn->blghp/dot_general | solution.py:721
  77.9 2.3 %copy.136 = f32[2,128,4,4,64]{4,3,2,1,0:T(4,128)S(1)} copy(f32[2,128,4,4,64]{1,4,3,2,0:T(8,128)} %get-tuple-element.258) | data formatting | bytes 2097152 | tf_op jit(solution)/shard_map/reshape | solution.py:727
  80.1 1.5 reshape.2004
  81.8 0.3 copy.125
  82.1 0.2 copy-done.15
  82.3 2.2 %multiply_convert_fusion.9.x = bf16[256,1024]{1,0:T(8,128)(2,1)} fusion(f32[256,1024]{1,0:T(8,128)S(1)} %copy.125, f32[256,1024]{1,0:T(8,128)S(1)} %reshape.2004, f32[1024]{0:T(1024)S(1)} %copy-done.15, bf16[256,1024]{1,0:T(8,128)(2,1)} %param.27), kind=kLoop, calls=%fused_computation.48 | loop fusion | flops 2359296 | bytes 3149824 | tf_op jit(solution)/shard_map/convert_element_type | solution.py:732
  84.5 17.8 %shard_map.184 = bf16[256,4096]{1,0:T(8,128)(2,1)} custom-call(bf16[256,1024]{1,0:T(8,128)(2,1)} %multiply_convert_fusion.9.x), custom_call_target="tpu_custom_call" | custom-call | tf_op jit(solution)/shard_map/pallas_call | solution.py:166
  102.4 4.8 %convolution_convert_fusion.1 = bf16[256,512]{1,0:T(8,128)(2,1)} fusion(bf16[256,4096]{1,0:T(8,128)(2,1)} %shard_map.184, bf16[4096,512]{1,0:T(8,128)(2,1)} %param.35), kind=kOutput, calls=%fused_computation.34 | convolution fusion | flops 1073872896 | bytes 6553600 | tf_op jit(solution)/shard_map/dot_general | solution.py:787
  107.2 6.7 %shard_map.185 = bf16[4,64,512]{2,1,0:T(8,128)(2,1)} custom-call(bf16[4,64,512]{2,1,0:T(8,128)(2,1)} %bitcast.268), custom_call_target="tpu_custom_call" | custom-call | tf_op jit(solution)/shard_map/pallas_call | solution.py:79
  113.9 1.0 convert_bitcast_fusion
  115.0 0.2 fusion.32
  115.4 0.1 eq.26
  115.6 0.2 reduce_window_sum.33
  115.8 0.2 select_reduce_fusion.1
  115.9 0.1 reduce_sum.69
  116.4 1.5 convolution_convert_fusion
  117.8 74.0 %shard_map.186 = bf16[8,32,2048]{2,1,0:T(8,128)(2,1)} custom-call(bf16[8,32,2048]{2,1,0:T(8,128)(2,1)} %bitcast.256, bf16[1,2048,1024]{2,1,0:T(8,128)(2,1)} %wgate.1, bf16[1,2048,1024]{2,1,0:T(8,128)(2,1)} %wup.1, bf16[1,1024,2048]{2,1,0:T(8,128)(2,1)} %wdown.1), custom_call_target="tpu_custom_call" | custom-call | tf_op jit(solution)/shard_map/pallas_call | solution.py:554
  191.9 2.6 %fusion = bf16[64,2048]{1,0:T(8,128)(2,1)} fusion(f32[64,256]{1,0:T(8,128)S(1)} %select_reduce_fusion, bf16[256,2048]{1,0:T(8,128)(2,1)} %bitcast.255, bf16[64,2048]{1,0:T(8,128)(2,1)S(1)} %get-tuple-element.206), kind=kOutput, calls=%fused_computation.8 | convolution fusion | flops 403046400 | bytes 1638400 | tf_op jit(solution)/shard_map/dot_general | solution.py:833
  (97 shorter events, 2.9 us)
Async XLA Ops:
  1.1 13.3 %copy-start.11 = (bf16[5,1024]{1,0:T(8,128)(2,1)S(1)}, bf16[5,1024]{1,0:T(8,128)(2,1)}, u32[]{:S(2)}) copy-start(bf16[5,1024]{1,0:T(8,128)(2,1)} %param.31) | copy-start | bytes 30724
  1.1 13.3 %copy-start.13 = (bf16[5,512]{1,0:T(8,128)(2,1)S(1)}, bf16[5,512]{1,0:T(8,128)(2,1)}, u32[]{:S(2)}) copy-start(bf16[5,512]{1,0:T(8,128)(2,1)} %param.33) | copy-start | bytes 15364
  1.1 13.3 %copy-start.14 = (bf16[5,512]{1,0:T(8,128)(2,1)S(1)}, bf16[5,512]{1,0:T(8,128)(2,1)}, u32[]{:S(2)}) copy-start(bf16[5,512]{1,0:T(8,128)(2,1)} %param.32) | copy-start | bytes 15364
  15.6 2.6 %copy-start.18 = (f32[2,16]{1,0:T(2,128)S(1)}, f32[2,16]{1,0:T(2,128)}, u32[]{:S(2)}) copy-start(f32[2,16]{1,0:T(2,128)} %param.29) | copy-start | bytes 388
  15.6 2.7 %copy-start.9 = (bf16[2,256,16]{1,2,0:T(8,128)(2,1)S(1)}, bf16[2,256,16]{1,2,0:T(8,128)(2,1)}, u32[]{:S(2)}) copy-start(bf16[2,256,16]{1,2,0:T(8,128)(2,1)} %param.28) | copy-start | bytes 49156
  15.6 2.6 %copy-start.10 = (f32[256,16]{0,1:T(8,128)S(1)}, f32[256,16]{0,1:T(8,128)}, u32[]{:S(2)}) copy-start(f32[256,16]{0,1:T(8,128)} %param.30) | copy-start | bytes 49156
  19.6 2.9 %copy-start.3 = (bf16[2,128,4,4,64]{1,0,4,3,2:T(2,128)(2,1)}, bf16[2,128,4,4,64]{1,0,4,3,2:T(2,128)(2,1)S(1)}, u32[]{:S(2)}) copy-start(bf16[2,128,4,4,64]{1,0,4,3,2:T(2,128)(2,1)S(1)} %squeeze.96) | copy-start | bytes 1572868
  23.1 2.0 %copy-start.1 = (f32[2,4,4,64,128]{4,3,2,1,0:T(8,128)}, f32[2,4,4,64,128]{4,3,2,1,0:T(8,128)S(1)}, u32[]{:S(2)}) copy-start(f32[2,4,4,64,128]{4,3,2,1,0:T(8,128)S(1)} %get-tuple-element.144) | copy-start | bytes 3145732
  25.1 1.1 copy-start.5
  26.3 1.0 copy-start.6
  46.0 20.3 %copy-start.7 = (bf16[256,512]{1,0:T(8,128)(2,1)S(1)}, bf16[256,512]{1,0:T(8,128)(2,1)}, u32[]{:S(2)}) copy-start(bf16[256,512]{1,0:T(8,128)(2,1)} %get-tuple-element.220) | copy-start | bytes 786436
  66.6 2.3 %copy-start.4 = (bf16[2,128,4,4,64]{1,0,4,3,2:T(2,128)(2,1)S(1)}, bf16[2,128,4,4,64]{1,0,4,3,2:T(2,128)(2,1)}, u32[]{:S(2)}) copy-start(bf16[2,128,4,4,64]{1,0,4,3,2:T(2,128)(2,1)} %copy-done.3) | copy-start | bytes 1572868
  69.9 1.4 copy-start.2
  73.0 1.7 copy-start
  81.6 0.7 copy-start.15
  107.2 7.8 %copy-start.8 = (bf16[64,2048]{1,0:T(8,128)(2,1)S(1)}, bf16[64,2048]{1,0:T(8,128)(2,1)}, u32[]{:S(2)}) copy-start(bf16[64,2048]{1,0:T(8,128)(2,1)} %param.23) | copy-start | bytes 786436
  107.2 8.0 %copy-start.16 = (s32[256,2]{0,1:T(2,128)S(1)}, s32[256,2]{0,1:T(2,128)}, u32[]{:S(2)}) copy-start(s32[256,2]{0,1:T(2,128)} %param.37) | copy-start | bytes 6148
  107.2 9.2 %copy-start.12 = (f32[2048]{0:T(1024)S(1)}, f32[2048]{0:T(1024)}, u32[]{:S(2)}) copy-start(f32[2048]{0:T(1024)} %param.36) | copy-start | bytes 24580
  117.8 74.0 %copy-start.17 = (f32[64,2]{0,1:T(2,128)S(1)}, f32[64,2]{0,1:T(2,128)}, u32[]{:S(2)}) copy-start(f32[64,2]{0,1:T(2,128)} %param.38) | copy-start | bytes 1540

commit v2 on v1

--- a/solution.py
+++ b/solution.py
@@ -11,6 +11,7 @@
 STATE = 128
 BLOCK = 128
 TAPS = 5
+LANES = 128
 
 
 epsilon = 1e-06
@@ -735,6 +736,335 @@
     return head_normed.reshape(tokens, head_count * HEAD_DIM)
 
 
+def mixer_kernel(
+    n, span, value, key, query, gate, raw, rate, extra, vfilter, kfilter, qfilter, gain, out,
+    hv, hk, hq, pad, vals, keys, queries, turned, column, lines, totals, inner, weight,
+    fin, met, came, gone, held, given, result,
+    esend, erecv, tsend, trecv, xsend, xrecv, zsend, zrecv, ysend, yrecv,
+):
+    me = lax.axis_index("sp")
+    b, a = lax.rem(me, 2), lax.div(me, 2)
+    beside, planes = me + 1 - 2 * b, n // 2
+    tokens, wide = value.shape
+    heads = raw.shape[2]
+    groups = key.shape[1] // STATE
+    tiles = wide // LANES
+    per = tiles // groups
+    half = tiles // 2
+    chunks = half // span
+    f32 = jnp.float32
+
+    edge = hv.shape[1]
+    arrays = [(value, hv), (key, hk), (query, hq)]
+
+    def edge_copy(i, way):
+        src, halo = arrays[i]
+        start, peer = (tokens - edge, lax.rem(me + 1, n)) if way == 0 else (0, lax.rem(me + n - 1, n))
+        return remote(
+            src.at[pl.ds(start, edge)], halo.at[way], esend.at[i, way], erecv.at[i, way], {"sp": peer}
+        )
+
+    greet([{"sp": lax.rem(me + d, n)} for d in range(1, n)])
+    sends = [me < n - 1, me > 0]
+    waits = [me > 0, me < n - 1]
+    for way in range(2):
+
+        @pl.when(sends[way])
+        def _():
+            for i in range(3):
+                edge_copy(i, way).start()
+
+        @pl.when(jnp.logical_not(waits[way]))
+        def _():
+            for _, halo in arrays:
+                halo[way] = jnp.zeros(halo.shape[1:], halo.dtype)
+
+    row = lax.broadcasted_iota(jnp.int32, (tokens, tokens), 0)
+    col = lax.broadcasted_iota(jnp.int32, (tokens, tokens), 1)
+    prefix = (col <= row).astype(f32)
+    column[...] = jnp.zeros(column.shape, f32)
+    lane = lax.broadcasted_iota(jnp.int32, (tokens, LANES), 1)
+    for d in range(2):
+        r = raw[d].astype(f32)
+        step = jnp.maximum(r, 0.0) + jnp.log1p(jnp.exp(-jnp.abs(r)))
+        decay = -jnp.exp(rate[pl.ds(d, 1), :]) * step + extra[...]
+        total = jnp.dot(prefix, decay, preferred_element_type=f32, precision=highest)
+        last = total[tokens - 1 : tokens, :]
+        part = total if d == 0 else total - decay
+        gap = last - total if d == 0 else part
+        read = total if d == 0 else last - part
+        column[d, :, 0:heads] = part
+        column[2 + d, :, 0:heads] = step
+        column[4 + d, :, 0:heads] = jnp.exp(gap) * step
+        column[6 + d, :, 0:heads] = jnp.exp(read)
+        totals[0, d, :, :] = jnp.zeros(totals.shape[2:], f32)
+        totals[0, d, :, 0:heads] = jnp.broadcast_to(jnp.exp(last), (8, heads))
+    for q in range(4):
+        lines[q] = column[q].T
+
+    def total_copy():
+        return remote(totals.at[0], totals.at[1], tsend.at[0], trecv.at[0], {"sp": beside})
+
+    total_copy().start()
+
+    for way in range(2):
+
+        @pl.when(waits[way])
+        def _():
+            for i in range(3):
+                edge_copy(i, way).wait_recv()
+
+    def convolve(src, halo, taps, store):
+        reach = (TAPS - 1) // 2
+
+        def step(i):
+            cols = pl.ds(pl.multiple_of(i * LANES, LANES), LANES)
+            pad[pl.ds(8, tokens)] = src[:, cols].astype(f32)
+            pad[pl.ds(0, 8)] = halo[0, :, cols].astype(f32)[edge - 8 :]
+            pad[pl.ds(8 + tokens, 8)] = halo[1, :, cols].astype(f32)[:8]
+            w = taps[:, cols].astype(f32)
+            acc = w[0:1] * pad[pl.ds(8 - reach, tokens)]
+            for o in range(1, TAPS):
+                acc = acc + w[o : o + 1] * pad[pl.ds(8 - reach + o, tokens)]
+            store(i, cols, acc)
+
+        each(src.shape[1] // LANES, step)
+
+    def silu(v):
+        return v / (1.0 + jnp.exp(-v))
+
+    def keep_values(i, cols, acc):
+        vals[:, cols] = acc.astype(vals.dtype)
+
+    def keep_keys(i, cols, acc):
+        acc = silu(acc)
+        keys[:, cols] = acc.astype(keys.dtype)
+        turned[i] = acc.T.astype(turned.dtype)
+
+    def keep_queries(i, cols, acc):
+        queries[:, cols] = silu(acc).astype(queries.dtype)
+
+    convolve(value, hv, vfilter, keep_values)
+    convolve(key, hk, kfilter, keep_keys)
+
+    def spread(x, k):
+        low, high = x[:, k : k + 1], x[:, k + 1 : k + 2]
+        return jnp.where(lane[: x.shape[0]] < HEAD_DIM, low, high)
+
+    def shifted(q, first):
+        return pltpu.roll(column[q], lax.rem(LANES - first, LANES), 1)
+
+    def cross(d, c):
+        spot = pl.ds((1 - b) * half + c * span, span)
+        mine = pl.ds(b * half + c * span, span)
+        return (
+            remote(fin.at[d, spot], met.at[d, pl.ds(c * span, span)], xsend.at[d, c], xrecv.at[d, c], {"sp": beside}),
+            mine,
+        )
+
+    def states(i):
+        g = lax.rem(i + (1 - b) * (groups // 2), groups)
+        for d in range(2):
+            scale = shifted(4 + d, g * 2 * per)
+            for k in range(per):
+                cols = pl.ds(pl.multiple_of((g * per + k) * LANES, LANES), LANES)
+                scaled = (vals[:, cols].astype(f32) * spread(scale, 2 * k)).astype(vals.dtype)
+                fin[d, g * per + k] = jnp.dot(
+                    turned[g], scaled, preferred_element_type=f32
+                ).astype(fin.dtype)
+
+    each(groups, states)
+    for c in range(chunks):
+        for d in range(2):
+            cross(d, c)[0].start()
+    convolve(query, hq, qfilter, keep_queries)
+
+    block_row = lax.broadcasted_iota(jnp.int32, (BLOCK, BLOCK), 0)
+    block_col = lax.broadcasted_iota(jnp.int32, (BLOCK, BLOCK), 1)
+
+    def within(g):
+        kcols = pl.ds(pl.multiple_of(g * STATE, STATE), STATE)
+        scores = lax.dot_general(
+            queries[:, kcols], keys[:, kcols], (((1,), (1,)), ((), ())), preferred_element_type=f32
+        )
+        first = g * 2 * per
+        ahead, behind = shifted(0, first), shifted(1, first)
+        for k in range(2 * per):
+            fr, er = lines[0, pl.ds(first + k, 1), :], lines[1, pl.ds(first + k, 1), :]
+            sf, sb = lines[2, pl.ds(first + k, 1), :], lines[3, pl.ds(first + k, 1), :]
+            for i in range(tokens // BLOCK):
+                rows = slice(i * BLOCK, (i + 1) * BLOCK)
+                fc = jnp.broadcast_to(ahead[rows, k : k + 1], (BLOCK, BLOCK))
+                ec = jnp.broadcast_to(behind[rows, k : k + 1], (BLOCK, BLOCK))
+                for m in range(tokens // BLOCK):
+                    cols = slice(m * BLOCK, (m + 1) * BLOCK)
+                    if m < i:
+                        gap, size = fc - fr[:, cols], sf[:, cols]
+                    elif m > i:
+                        gap, size = er[:, cols] - ec, sb[:, cols]
+                    else:
+                        lower, upper = block_col <= block_row, block_col >= block_row
+                        gap = jnp.where(lower, fc - fr[:, cols], er[:, cols] - ec)
+                        size = jnp.where(lower, sf[:, cols], 0.0) + jnp.where(upper, sb[:, cols], 0.0)
+                    weight[k % 2, rows, cols] = (scores[rows, cols] * jnp.exp(gap) * size).astype(
+                        weight.dtype
+                    )
+            if k % 2 == 1:
+                spot = pl.ds(pl.multiple_of((g * per + k // 2) * LANES, LANES), LANES)
+                both = vals[:, spot]
+                low = jnp.dot(weight[0], both, preferred_element_type=f32)
+                high = jnp.dot(weight[1], both, preferred_element_type=f32)
+                inner[:, spot] = jnp.where(lane < HEAD_DIM, low, high)
+
+    each(groups, within)
+
+    total_copy().wait()
+    factor = [pltpu.roll(totals[i, d], lax.rem(LANES - 2 * b * half, LANES), 1) for i in range(2) for d in range(2)]
+    early = b == 0
+
+    def chain(d, c):
+        peer = lax.rem(me + (2 if d == 0 else n - 2), n)
+        spot = pl.ds(c * span, span)
+        return remote(gone.at[d, spot], came.at[d, spot], zsend.at[d, c], zrecv.at[d, c], {"sp": peer})
+
+    def answer(d, c):
+        there = pl.ds(b * half + c * span, span)
+        return remote(
+            given.at[d, pl.ds(c * span, span)], result.at[d, there], ysend.at[d, c], yrecv.at[d, c], {"sp": beside}
+        )
+
+    def answered(d, c):
+        there = pl.ds((1 - b) * half + c * span, span)
+        return remote(
+            given.at[d, pl.ds(c * span, span)], result.at[d, there], ysend.at[d, c], yrecv.at[d, c], {"sp": beside}
+        )
+
+    for c in range(chunks):
+        for d in range(2):
+            cross(d, c)[0].wait_recv()
+            starts = a == 0 if d == 0 else a == planes - 1
+            ends = a == planes - 1 if d == 0 else a == 0
+
+            @pl.when(starts)
+            def _():
+                came[d, pl.ds(c * span, span)] = jnp.zeros((span,) + came.shape[2:], came.dtype)
+
+            @pl.when(jnp.logical_not(starts))
+            def _():
+                chain(d, c).wait_recv()
+
+            for k in range(span):
+                u = c * span + k
+                mine = spread(factor[d], 2 * u)[0:1]
+                other = spread(factor[2 + d], 2 * u)[0:1]
+                state = came[d, u].astype(f32)
+                own = fin[d, b * half + u].astype(f32)
+                got = met[d, u].astype(f32)
+                near_first = early if d == 0 else jnp.logical_not(early)
+                head = jnp.where(near_first, own, got)
+                tail = jnp.where(near_first, got, own)
+                head_factor = jnp.where(near_first, mine, other)
+                tail_factor = jnp.where(near_first, other, mine)
+                middle = head_factor * state + head
+                gone[d, u] = (tail_factor * middle + tail).astype(gone.dtype)
+                held[d, u] = jnp.where(near_first, state, middle).astype(held.dtype)
+                given[d, u] = jnp.where(near_first, middle, state).astype(given.dtype)
+
+            @pl.when(jnp.logical_not(ends))
+            def _():
+                chain(d, c).start()
+
+            answer(d, c).start()
+            result[d, pl.ds(b * half + c * span, span)] = held[d, pl.ds(c * span, span)]
+
+    block = lax.broadcasted_iota(jnp.int32, (LANES, LANES), 0) // HEAD_DIM
+    share = jnp.where(
+        block == lax.broadcasted_iota(jnp.int32, (LANES, LANES), 1) // HEAD_DIM, 1.0 / HEAD_DIM, 0.0
+    ).astype(vals.dtype)
+
+    def finish(u):
+        g = lax.div(u, per)
+        kcols = pl.ds(pl.multiple_of(g * STATE, STATE), STATE)
+        cols = pl.ds(pl.multiple_of(u * LANES, LANES), LANES)
+        q = queries[:, kcols]
+        mixed = inner[:, cols]
+        for d in range(2):
+            carried = jnp.dot(q, result[d, u], preferred_element_type=f32)
+            mixed = mixed + spread(shifted(6 + d, 2 * u), 0) * carried
+        gated = mixed * silu(gate[:, cols].astype(f32))
+        square = gated * gated
+        top = square.astype(share.dtype)
+        rest = (square - top.astype(f32)).astype(share.dtype)
+        mean = jnp.dot(top, share, preferred_element_type=f32)
+        mean = mean + jnp.dot(rest, share, preferred_element_type=f32)
+        out[:, cols] = (gated * lax.rsqrt(mean + epsilon) * gain[:, cols]).astype(out.dtype)
+
+    each(half, lambda u: finish(b * half + u))
+    for c in range(chunks):
+        for d in range(2):
+            answered(d, c).wait_recv()
+    each(half, lambda u: finish((1 - b) * half + u))
+
+    for way in range(2):
+
+        @pl.when(sends[way])
+        def _():
+            for i in range(3):
+                edge_copy(i, way).wait_send()
+
+    for c in range(chunks):
+        for d in range(2):
+            ends = a == planes - 1 if d == 0 else a == 0
+            cross(d, c)[0].wait_send()
+            answer(d, c).wait_send()
+
+            @pl.when(jnp.logical_not(ends))
+            def _():
+                chain(d, c).wait_send()
+
+
+def run_mixer(
+    value, key, query, gate, raw, rate, extra, vfilter, kfilter, qfilter, gain, number
+):
+    n = lax.axis_size("sp")
+    tokens, wide = value.shape
+    narrow = key.shape[1]
+    groups, tiles = narrow // STATE, wide // LANES
+    half = tiles // 2
+    span = 2 if half % 2 == 0 else 1
+    kind, f32 = value.dtype, jnp.float32
+    edge = 16
+    state = pltpu.VMEM((2, half, STATE, LANES), kind)
+    full = pltpu.VMEM((2, tiles, STATE, LANES), kind)
+    sems = dma(2, half // span)
+    return pl.pallas_call(
+        functools.partial(mixer_kernel, n, span),
+        out_shape=jax.ShapeDtypeStruct((tokens, wide), kind),
+        in_specs=vmem(11),
+        out_specs=vmem(1)[0],
+        scratch_shapes=[
+            pltpu.VMEM((2, edge, wide), kind),
+            pltpu.VMEM((2, edge, narrow), kind),
+            pltpu.VMEM((2, edge, narrow), kind),
+            pltpu.VMEM((tokens + 16, LANES), f32),
+            pltpu.VMEM((tokens, wide), kind),
+            pltpu.VMEM((tokens, narrow), kind),
+            pltpu.VMEM((tokens, narrow), kind),
+            pltpu.VMEM((groups, STATE, tokens), kind),
+            pltpu.VMEM((8, tokens, LANES), f32),
+            pltpu.VMEM((4, LANES, tokens), f32),
+            pltpu.VMEM((2, 2, 8, LANES), f32),
+            pltpu.VMEM((tokens, wide), f32),
+            pltpu.VMEM((2, tokens, tokens), kind),
+            full, state, state, state, state, state, full,
+            dma(3, 2), dma(3, 2), dma(1), dma(1), sems, sems, sems, sems, sems, sems,
+        ],
+        compiler_params=pltpu.CompilerParams(
+            collective_id=number, has_side_effects=True, vmem_limit_bytes=40 * 2**20
+        ),
+    )(value, key, query, gate, raw, rate, extra, vfilter, kfilter, qfilter, gain.reshape(1, -1))
+
+
 def slot_table(route_rows, experts, capacity):
     flat_ids = route_rows.reshape(-1)
     expert_ids = lax.broadcasted_iota(jnp.int32, (flat_ids.shape[0], experts), 1)
@@ -771,7 +1101,7 @@
     expert_up_matrix,
     expert_down_matrix,
 ):
-    heads_out = mix_tokens(
+    operands = (
         value_projected,
         key_projected,
         query_projected,
@@ -784,6 +1114,10 @@
         query_filter_weight,
         head_norm_gain,
     )
+    if value_projected.shape[1] % (2 * LANES) == 0 and lax.axis_size("sp") % 2 == 0:
+        heads_out = run_mixer(*operands, 2)
+    else:
+        heads_out = mix_tokens(*operands)
     projected = jnp.dot(
         gather_columns(heads_out, 4),
         mixer_output_matrix,

time: 198 us -> 187 us (0.944)
  Pallas kernels: 139 us -> 161 us
  other arithmetic: 15.5 us -> 2.59 us
  matrix products: 19.1 us -> 8.89 us
  local copies, waits for them, and re-layouts: 19.7 us -> 11.2 us
    pallas_call x1, Pallas kernels: 9.52 us -> 64.8 us  [run_mixer(): pl.pallas_call(functools.partial(mixer_kernel, n, span), out_shape=jax.Sh...]
    pallas_call x3 -> x1, Pallas kernels: 37.9 us -> 6.69 us  [exchange(): pl.pallas_call(functools.partial(exchange_kernel, axis, n, k), out_shape=...]
    dot_general x8 -> x0, matrix products: 10.3 us -> none  [the longest x1 3.15 us: mix_tokens(): jnp.einsum('blgn,bghpn->blghp', query_rows, backward_in.astype(jnp.bfloat...]
    unnamed x43 -> x28, local copies, waits for them, and re-layouts: 2.84 us -> 9.92 us
    reshape x7 -> x0, local copies, waits for them, and re-layouts: 7.04 us -> none  [the longest x2 3.77 us: mix_tokens(): (inner + forward_read + backward_read).reshape(tokens, head_count, HEAD_DIM)]
    convert_element_type x5 -> x0, other arithmetic: 4.87 us -> none  [the longest x1 2.22 us: mix_tokens(): (gated * inverse_rms * head_norm_gain.reshape(head_count, HEAD_DIM)).asty...]
    slice x3 -> x0, local copies, waits for them, and re-layouts: 2.81 us -> none  [the longest x1 1.93 us: carried_states(): return (both[:, 0].reshape(shape), both[:, 1].reshape(shape))]
    another operation x7 -> x0, other arithmetic: 2.4 us -> none
where the time goes in v2:
time: 187 us; the launch traced here: 184 us
  Pallas kernels  161 us (86%)
  local copies, waits for them, and re-layouts  11.2 us (6%)
  matrix products  8.89 us (5%)
  other arithmetic  2.59 us (1%)
    pallas_call x1, Pallas kernels, run_experts(): pl.pallas_call(functools.partial(expert_kernel, sp, tp), out_shape=jax.Sh...  71.9 us
    pallas_call x1, Pallas kernels, run_mixer(): pl.pallas_call(functools.partial(mixer_kernel, n, span), out_shape=jax.Sh...  64.8 us
    pallas_call x1, Pallas kernels, gather_columns(): pl.pallas_call(functools.partial(gather_kernel, tp, pieces), out_shape=ja...  17.9 us
    unnamed x28, local copies, waits for them, and re-layouts  9.92 us
    pallas_call x1, Pallas kernels, exchange(): pl.pallas_call(functools.partial(exchange_kernel, axis, n, k), out_shape=...  6.69 us
    dot_general x1, matrix products, shards(): jnp.dot(gather_columns(heads_out, 4), mixer_output_matrix, preferred_elem...  4.81 us

profile of v2, /device:TPU:0, one launch (start us, length us, event | category | flops | bytes accessed | tf_op | source)
XLA Modules:
  0.0 184.0 jit_solution(12971701940040536823)
XLA Ops:
  0.0 0.7 constant_dynamic-slice_fusion
  0.8 0.1 copy.38
  0.8 0.1 eq.26
  1.0 0.1 fusion.7
  1.1 0.2 reduce_window_sum.11
  1.3 0.2 select_reduce_fusion.1
  1.4 0.1 reduce_sum.39
  1.6 0.1 copy.39
  1.7 0.8 multiply_add_fusion
  2.4 0.1 convert_reduce_fusion
  2.5 0.8 copy.35.raw
  3.4 0.8 copy.36.extra
  4.2 0.0 copy-start.1
  4.2 1.0 copy-done.1
  5.2 0.0 copy-start.2
  5.2 1.0 copy-done.2
  6.3 0.0 copy-start.3
  6.3 0.9 copy-done.3
  7.2 0.0 copy-start.4
  7.2 0.9 copy-done.4
  8.2 0.0 copy-start.5
  8.2 0.7 copy-done.5
  8.9 0.0 copy-start.6
  8.9 0.7 copy-done.6
  9.6 0.0 copy-start.7
  9.6 0.7 copy-done.7
  10.3 0.0 copy-start.8
  10.3 0.7 copy-done.8
  11.0 0.0 copy-start.9
  11.0 0.7 copy-done.9
  11.7 64.8 %shard_map.181.x = bf16[256,1024]{1,0:T(8,128)(2,1)S(1)} custom-call(bf16[256,1024]{1,0:T(8,128)(2,1)S(1)} %copy-done.1, bf16[256,512]{1,0:T(8,128)(2,1)S(1)} %copy-done.3, bf16[256,512]{1,0:T(8,128)(2,1)S(1)} %copy-done.4, bf16[256,1024]{1,0:T(8,128)(2,1)S(1)} %copy-done.2, bf16[2,256,16]{2,1,0:T(8,128)(2,1)S(1)} %copy.35.raw, f32[2,16]{1,0:T(2,128)S(1)} %copy-done.9, ...), custom_call_target="tpu_custom_call" | custom-call | tf_op jit(solution)/shard_map/pallas_call | solution.py:1040
  76.5 0.0 copy-start
  76.5 0.8 copy-done
  77.3 17.9 %shard_map.182 = bf16[256,4096]{1,0:T(8,128)(2,1)} custom-call(bf16[256,1024]{1,0:T(8,128)(2,1)} %copy-done), custom_call_target="tpu_custom_call" | custom-call | tf_op jit(solution)/shard_map/pallas_call | solution.py:167
  95.1 0.0 copy-start.10
  95.2 0.0 copy-start.11
  95.2 4.8 %convolution_convert_fusion.1 = bf16[256,512]{1,0:T(8,128)(2,1)} fusion(bf16[256,4096]{1,0:T(8,128)(2,1)} %shard_map.182, bf16[4096,512]{1,0:T(8,128)(2,1)} %param.31), kind=kOutput, calls=%fused_computation.3 | convolution fusion | flops 1073872896 | bytes 6553600 | tf_op jit(solution)/shard_map/dot_general | solution.py:1121
  100.0 6.7 %shard_map.183 = bf16[4,64,512]{2,1,0:T(8,128)(2,1)} custom-call(bf16[4,64,512]{2,1,0:T(8,128)(2,1)} %bitcast.17), custom_call_target="tpu_custom_call" | custom-call | tf_op jit(solution)/shard_map/pallas_call | solution.py:80
  106.7 1.0 convert_bitcast_fusion
  107.7 0.0 copy-done.10
  107.7 0.2 fusion.1
  107.9 0.0 copy-done.11
  107.9 1.5 convolution_convert_fusion
  109.4 0.0 copy-start.12
  109.4 71.9 %shard_map.184 = bf16[8,32,2048]{2,1,0:T(8,128)(2,1)} custom-call(bf16[8,32,2048]{2,1,0:T(8,128)(2,1)} %bitcast.15, bf16[1,2048,1024]{2,1,0:T(8,128)(2,1)} %wgate.1, bf16[1,2048,1024]{2,1,0:T(8,128)(2,1)} %wup.1, bf16[1,1024,2048]{2,1,0:T(8,128)(2,1)} %wdown.1), custom_call_target="tpu_custom_call" | custom-call | tf_op jit(solution)/shard_map/pallas_call | solution.py:555
  181.3 0.0 copy-done.12
  181.3 0.1 select_reduce_fusion
  181.4 2.6 %fusion = bf16[64,2048]{1,0:T(8,128)(2,1)} fusion(f32[64,256]{1,0:T(8,128)S(1)} %select_reduce_fusion, bf16[256,2048]{1,0:T(8,128)(2,1)} %bitcast.14, bf16[64,2048]{1,0:T(8,128)(2,1)S(1)} %get-tuple-element.6), kind=kOutput, calls=%fused_computation.2 | convolution fusion | flops 403046400 | bytes 1638400 | tf_op jit(solution)/shard_map/dot_general | solution.py:1167
  (2 shorter events, 0.0 us)
Async XLA Ops:
  4.2 1.0 copy-start.1
  5.2 1.0 copy-start.2
  6.3 0.9 copy-start.3
  7.2 0.9 copy-start.4
  8.2 0.7 copy-start.5
  8.9 0.7 copy-start.6
  9.6 0.7 copy-start.7
  10.3 0.7 copy-start.8
  11.0 0.7 copy-start.9
  76.5 0.8 copy-start
  95.1 12.6 %copy-start.10 = (bf16[64,2048]{1,0:T(8,128)(2,1)S(1)}, bf16[64,2048]{1,0:T(8,128)(2,1)}, u32[]{:S(2)}) copy-start(bf16[64,2048]{1,0:T(8,128)(2,1)} %param.19) | copy-start | bytes 786436
  95.2 12.8 %copy-start.11 = (f32[2048]{0:T(1024)S(1)}, f32[2048]{0:T(1024)}, u32[]{:S(2)}) copy-start(f32[2048]{0:T(1024)} %param.32) | copy-start | bytes 24580
  109.4 71.9 %copy-start.12 = (f32[64,2]{0,1:T(2,128)S(1)}, f32[64,2]{0,1:T(2,128)}, u32[]{:S(2)}) copy-start(f32[64,2]{0,1:T(2,128)} %param.34) | copy-start | bytes 1540

commit v3 on v2

--- a/solution.py
+++ b/solution.py
@@ -473,7 +473,7 @@
             back(d).start()
 
     tile = min(ff, 256)
-    wide = min(width, 256)
+    wide = min(width, 512)
 
     def gate_up(g):
         base = flip(me, 2 * g) - lax.rem(flip(me, 2 * g), 2)
@@ -497,40 +497,70 @@
 
         each(width // wide, step)
 
-    for d in range(1, sp):
+    order = [0, 1] + list(range(2, sp // 2))[::-1]
+    line = [d for g in order for d in (2 * g, 2 * g + 1)]
+    for d in line[1:]:
         across(d).start()
     ahead = min(4, sp)
-    onward(0)
-    onward(1)
-    onward(2)
-    pass_on(0)
-    onward(3)
-    pass_on(1)
+    with jax.named_scope('prologue'):
+        onward(0)
+        onward(1)
+        onward(2)
+        pass_on(0)
+        onward(3)
+        pass_on(1)
     for copy in loads[:2]:
         copy.wait()
-    for g in range(sp // 2):
-        for d in (2 * g, 2 * g + 1):
-            if g > 0:
-                pass_on(d)
-        for d in (2 * g, 2 * g + 1):
-            for k in range(chips):
-                relay(d, k).wait_recv()
-        gate_up(g)
-        for d in (2 * g + ahead, 2 * g + ahead + 1):
-            if d < sp:
-                onward(d)
-        if g == 0:
+    count = len(order)
+    near = line[2:4] + line[:2] if count > 2 else line[:2]
+
+    def collect(ds):
+        for d in ds:
+            begin(d)
+        with jax.named_scope('join'):
+            for d in ds:
+                join(d)
+
+    def settle(ds):
+        with jax.named_scope('close'):
+            for d in ds:
+                close(d)
+
+    def carry(p):
+        if p + 2 < sp:
+            with jax.named_scope('onward'):
+                onward(line[p + 2])
+        if p < sp:
+            with jax.named_scope('pass'):
+                pass_on(line[p])
+
+    sent, closed = [], 0
+    for i, g in enumerate(order):
+        with jax.named_scope('relayw'):
+            for d in line[2 * i : 2 * i + 2]:
+                for k in range(chips):
+                    relay(d, k).wait_recv()
+        with jax.named_scope('gateup'):
+            gate_up(g)
+        carry(2 * i + 2)
+        settle(sent[closed : closed + 2])
+        closed = min(len(sent), closed + 2)
+        if i == 0:
             loads[2].wait()
-        down(g)
-        begin(2 * g)
-        begin(2 * g + 1)
-        if g > 0:
-            close(2 * g - 2)
-            close(2 * g - 1)
-        join(2 * g)
-        join(2 * g + 1)
-    close(sp - 2)
-    close(sp - 1)
+        with jax.named_scope('down'):
+            down(g)
+        carry(2 * i + 3)
+        ds = line[2 * i : 2 * i + 2]
+        if i == count - 1:
+            ds = ds + near if ds[0] not in near else near[2:] + ds + near[:2]
+            ds = [d for d in ds if d not in sent]
+        elif i >= 2:
+            ds = ds + [near.pop(0)] if len(near) > 3 else ds
+        elif i < 2:
+            ds = []
+        collect(ds)
+        sent = sent + ds
+    settle(sent[closed:])
     for d in range(sp):
         for k in range(1, chips):
             forward(d, k).wait_send()
@@ -737,16 +767,29 @@
 
 
 def mixer_kernel(
-    n, span, value, key, query, gate, raw, rate, extra, vfilter, kfilter, qfilter, gain, out,
+    n, span, far_value, far_key, far_query, far_gate, far_raw, far_rate, far_extra,
+    far_vfilter, far_kfilter, far_qfilter, far_gain, far_matrix, out,
+    value, key, query, gate, raw, rate, extra, vfilter, kfilter, qfilter, gain, matrix,
     hv, hk, hq, pad, vals, keys, queries, turned, column, lines, totals, inner, weight,
-    fin, met, came, gone, held, given, result,
-    esend, erecv, tsend, trecv, xsend, xrecv, zsend, zrecv, ysend, yrecv,
+    fin, met, came, gone, given, result,
+    gathered, product, mine, theirs,
+    esend, erecv, tsend, trecv, xsend, xrecv, zsend, zrecv, ysend, yrecv, load,
+    fsend, frecv, rsend, rrecv, psend, precv,
 ):
+    far = [far_value, far_key, far_query, far_raw, far_rate, far_extra, far_vfilter, far_kfilter,
+           far_qfilter, far_gain, far_gate, far_matrix]
+    near = [value, key, query, raw, rate, extra, vfilter, kfilter, qfilter, gain, gate, matrix]
+    loads = [pltpu.make_async_copy(far[i], near[i], load.at[i]) for i in range(len(far))]
+    for copy in loads:
+        copy.start()
     me = lax.axis_index("sp")
     b, a = lax.rem(me, 2), lax.div(me, 2)
     beside, planes = me + 1 - 2 * b, n // 2
+    tp = gathered.shape[0]
+    j, chip, core, chips, partner = tp_places(tp)
+    others = [lax.rem(chip + d, chips) * 2 + core for d in range(1, chips)]
     tokens, wide = value.shape
-    heads = raw.shape[2]
+    heads = raw.shape[1]
     groups = key.shape[1] // STATE
     tiles = wide // LANES
     per = tiles // groups
@@ -764,7 +807,13 @@
             src.at[pl.ds(start, edge)], halo.at[way], esend.at[i, way], erecv.at[i, way], {"sp": peer}
         )
 
-    greet([{"sp": lax.rem(me + d, n)} for d in range(1, n)])
+    with jax.named_scope('greet'):
+        greet(
+            [{"sp": lax.rem(me + d, n)} for d in range(1, n)]
+            + [{"tp": lax.rem(j + d, tp)} for d in range(1, tp)]
+        )
+    for copy in loads[:3]:
+        copy.wait()
     sends = [me < n - 1, me > 0]
     waits = [me > 0, me < n - 1]
     for way in range(2):
@@ -779,28 +828,36 @@
             for _, halo in arrays:
                 halo[way] = jnp.zeros(halo.shape[1:], halo.dtype)
 
+    for copy in loads[3:-2]:
+        copy.wait()
     row = lax.broadcasted_iota(jnp.int32, (tokens, tokens), 0)
     col = lax.broadcasted_iota(jnp.int32, (tokens, tokens), 1)
-    prefix = (col <= row).astype(f32)
-    column[...] = jnp.zeros(column.shape, f32)
+    prefix = (row <= col).astype(f32)
     lane = lax.broadcasted_iota(jnp.int32, (tokens, LANES), 1)
+    lines[...] = jnp.zeros(lines.shape, f32)
+    same_head = lax.broadcasted_iota(jnp.int32, (heads, heads), 0) == lax.broadcasted_iota(
+        jnp.int32, (heads, heads), 1
+    )
+
+    def keep_line(q, x):
+        lines[pl.ds(q * heads, heads), :] = x
+
     for d in range(2):
         r = raw[d].astype(f32)
         step = jnp.maximum(r, 0.0) + jnp.log1p(jnp.exp(-jnp.abs(r)))
-        decay = -jnp.exp(rate[pl.ds(d, 1), :]) * step + extra[...]
-        total = jnp.dot(prefix, decay, preferred_element_type=f32, precision=highest)
-        last = total[tokens - 1 : tokens, :]
+        across_heads = jnp.broadcast_to(-jnp.exp(rate[pl.ds(d, 1), :]), (heads, heads))
+        speed = jnp.sum(jnp.where(same_head, across_heads, 0.0), axis=1, keepdims=True)
+        decay = speed * step + extra[...]
+        total = jnp.dot(decay, prefix, preferred_element_type=f32, precision=highest)
+        last = total[:, tokens - 1 : tokens]
         part = total if d == 0 else total - decay
-        gap = last - total if d == 0 else part
-        read = total if d == 0 else last - part
-        column[d, :, 0:heads] = part
-        column[2 + d, :, 0:heads] = step
-        column[4 + d, :, 0:heads] = jnp.exp(gap) * step
-        column[6 + d, :, 0:heads] = jnp.exp(read)
-        totals[0, d, :, :] = jnp.zeros(totals.shape[2:], f32)
-        totals[0, d, :, 0:heads] = jnp.broadcast_to(jnp.exp(last), (8, heads))
-    for q in range(4):
-        lines[q] = column[q].T
+        keep_line(d, part)
+        keep_line(2 + d, step)
+        keep_line(4 + d, jnp.exp(last - total if d == 0 else part) * step)
+        keep_line(6 + d, jnp.exp(total if d == 0 else last - part))
+    column[...] = lines[...].T
+    totals[0, 0] = jnp.broadcast_to(column[tokens - 1 : tokens, :], totals.shape[2:])
+    totals[0, 1] = jnp.broadcast_to(column[0:1, :], totals.shape[2:])
 
     def total_copy():
         return remote(totals.at[0], totals.at[1], tsend.at[0], trecv.at[0], {"sp": beside})
@@ -844,22 +901,21 @@
     def keep_queries(i, cols, acc):
         queries[:, cols] = silu(acc).astype(queries.dtype)
 
-    convolve(value, hv, vfilter, keep_values)
-    convolve(key, hk, kfilter, keep_keys)
+    with jax.named_scope('conv'):
+        convolve(value, hv, vfilter, keep_values)
+        convolve(key, hk, kfilter, keep_keys)
 
     def spread(x, k):
         low, high = x[:, k : k + 1], x[:, k + 1 : k + 2]
         return jnp.where(lane[: x.shape[0]] < HEAD_DIM, low, high)
 
     def shifted(q, first):
-        return pltpu.roll(column[q], lax.rem(LANES - first, LANES), 1)
+        return pltpu.roll(column[...], lax.rem(2 * LANES - q * heads - first, LANES), 1)
 
     def cross(d, c):
         spot = pl.ds((1 - b) * half + c * span, span)
-        mine = pl.ds(b * half + c * span, span)
-        return (
-            remote(fin.at[d, spot], met.at[d, pl.ds(c * span, span)], xsend.at[d, c], xrecv.at[d, c], {"sp": beside}),
-            mine,
+        return remote(
+            fin.at[d, spot], met.at[d, pl.ds(c * span, span)], xsend.at[d, c], xrecv.at[d, c], {"sp": beside}
         )
 
     def states(i):
@@ -873,11 +929,13 @@
                     turned[g], scaled, preferred_element_type=f32
                 ).astype(fin.dtype)
 
-    each(groups, states)
+    with jax.named_scope('states'):
+        each(groups, states)
     for c in range(chunks):
         for d in range(2):
-            cross(d, c)[0].start()
-    convolve(query, hq, qfilter, keep_queries)
+            cross(d, c).start()
+    with jax.named_scope('convq'):
+        convolve(query, hq, qfilter, keep_queries)
 
     block_row = lax.broadcasted_iota(jnp.int32, (BLOCK, BLOCK), 0)
     block_col = lax.broadcasted_iota(jnp.int32, (BLOCK, BLOCK), 1)
@@ -890,8 +948,8 @@
         first = g * 2 * per
         ahead, behind = shifted(0, first), shifted(1, first)
         for k in range(2 * per):
-            fr, er = lines[0, pl.ds(first + k, 1), :], lines[1, pl.ds(first + k, 1), :]
-            sf, sb = lines[2, pl.ds(first + k, 1), :], lines[3, pl.ds(first + k, 1), :]
+            fr, er = lines[pl.ds(0 * heads + first + k, 1), :], lines[pl.ds(1 * heads + first + k, 1), :]
+            sf, sb = lines[pl.ds(2 * heads + first + k, 1), :], lines[pl.ds(3 * heads + first + k, 1), :]
             for i in range(tokens // BLOCK):
                 rows = slice(i * BLOCK, (i + 1) * BLOCK)
                 fc = jnp.broadcast_to(ahead[rows, k : k + 1], (BLOCK, BLOCK))
@@ -916,66 +974,69 @@
                 high = jnp.dot(weight[1], both, preferred_element_type=f32)
                 inner[:, spot] = jnp.where(lane < HEAD_DIM, low, high)
 
-    each(groups, within)
-
-    total_copy().wait()
-    factor = [pltpu.roll(totals[i, d], lax.rem(LANES - 2 * b * half, LANES), 1) for i in range(2) for d in range(2)]
+    with jax.named_scope('within'):
+        each(groups, within)
+
+    with jax.named_scope('totw'):
+        total_copy().wait()
     early = b == 0
+    count = 2 * half
 
     def chain(d, c):
-        peer = lax.rem(me + (2 if d == 0 else n - 2), n)
+        peer = lax.rem(me + n + 2 - 4 * d, n)
         spot = pl.ds(c * span, span)
         return remote(gone.at[d, spot], came.at[d, spot], zsend.at[d, c], zrecv.at[d, c], {"sp": peer})
 
-    def answer(d, c):
-        there = pl.ds(b * half + c * span, span)
+    def answer(d, c, side):
+        there = pl.ds(side * half + c * span, span)
         return remote(
             given.at[d, pl.ds(c * span, span)], result.at[d, there], ysend.at[d, c], yrecv.at[d, c], {"sp": beside}
         )
 
-    def answered(d, c):
-        there = pl.ds((1 - b) * half + c * span, span)
-        return remote(
-            given.at[d, pl.ds(c * span, span)], result.at[d, there], ysend.at[d, c], yrecv.at[d, c], {"sp": beside}
-        )
-
-    for c in range(chunks):
-        for d in range(2):
-            cross(d, c)[0].wait_recv()
-            starts = a == 0 if d == 0 else a == planes - 1
-            ends = a == planes - 1 if d == 0 else a == 0
-
-            @pl.when(starts)
-            def _():
-                came[d, pl.ds(c * span, span)] = jnp.zeros((span,) + came.shape[2:], came.dtype)
-
-            @pl.when(jnp.logical_not(starts))
-            def _():
+    def link(d, c):
+        with jax.named_scope('crossw'):
+            cross(d, c).wait_recv()
+        starts = a == d * (planes - 1)
+        ends = a == (1 - d) * (planes - 1)
+
+        @pl.when(starts)
+        def _():
+            came[d, pl.ds(c * span, span)] = jnp.zeros((span,) + came.shape[2:], came.dtype)
+
+        @pl.when(jnp.logical_not(starts))
+        def _():
+            with jax.named_scope('chainw'):
                 chain(d, c).wait_recv()
 
-            for k in range(span):
-                u = c * span + k
-                mine = spread(factor[d], 2 * u)[0:1]
-                other = spread(factor[2 + d], 2 * u)[0:1]
-                state = came[d, u].astype(f32)
-                own = fin[d, b * half + u].astype(f32)
-                got = met[d, u].astype(f32)
-                near_first = early if d == 0 else jnp.logical_not(early)
-                head = jnp.where(near_first, own, got)
-                tail = jnp.where(near_first, got, own)
-                head_factor = jnp.where(near_first, mine, other)
-                tail_factor = jnp.where(near_first, other, mine)
-                middle = head_factor * state + head
-                gone[d, u] = (tail_factor * middle + tail).astype(gone.dtype)
-                held[d, u] = jnp.where(near_first, state, middle).astype(held.dtype)
-                given[d, u] = jnp.where(near_first, middle, state).astype(given.dtype)
-
-            @pl.when(jnp.logical_not(ends))
-            def _():
-                chain(d, c).start()
-
-            answer(d, c).start()
-            result[d, pl.ds(b * half + c * span, span)] = held[d, pl.ds(c * span, span)]
+        near_first = b == d
+        turn = lax.rem(2 * LANES - (6 + d) * heads - b * count, LANES)
+        ours = pltpu.roll(totals[0, d], turn, 1)
+        theirs = pltpu.roll(totals[1, d], turn, 1)
+        for k in range(span):
+            u = c * span + k
+            mine, other = spread(ours, 2 * u)[0:1], spread(theirs, 2 * u)[0:1]
+            state = came[d, u].astype(f32)
+            own = fin[d, b * half + u].astype(f32)
+            got = met[d, u].astype(f32)
+            head = jnp.where(near_first, own, got)
+            tail = jnp.where(near_first, got, own)
+            head_factor = jnp.where(near_first, mine, other)
+            tail_factor = jnp.where(near_first, other, mine)
+            middle = head_factor * state + head
+            gone[d, u] = (tail_factor * middle + tail).astype(gone.dtype)
+            result[d, b * half + u] = jnp.where(near_first, state, middle).astype(result.dtype)
+            given[d, u] = jnp.where(near_first, middle, state).astype(given.dtype)
+
+        @pl.when(jnp.logical_not(ends))
+        def _():
+            chain(d, c).start()
+
+        answer(d, c, b).start()
+
+    late = jnp.where(2 * a < planes, 0, 1)
+    for i in range(2):
+        for c in range(chunks):
+            link(late + i - 2 * late * i, c)
 
     block = lax.broadcasted_iota(jnp.int32, (LANES, LANES), 0) // HEAD_DIM
     share = jnp.where(
@@ -997,13 +1058,105 @@
         rest = (square - top.astype(f32)).astype(share.dtype)
         mean = jnp.dot(top, share, preferred_element_type=f32)
         mean = mean + jnp.dot(rest, share, preferred_element_type=f32)
-        out[:, cols] = (gated * lax.rsqrt(mean + epsilon) * gain[:, cols]).astype(out.dtype)
-
-    each(half, lambda u: finish(b * half + u))
+        gathered[j, u] = (gated * lax.rsqrt(mean + epsilon) * gain[:, cols]).astype(gathered.dtype)
+
+    def place(i):
+        return lax.rem(b * half + i, tiles)
+
+    def forward(i, k):
+        spot = gathered.at[j, place(i)]
+        return remote(spot, spot, fsend.at[i, k], frecv.at[i, k], {"tp": others[k - 1]})
+
+    def source(k):
+        return lax.rem(chip + chips - k, chips) * 2 + core
+
+    def relay(i, k):
+        spot = gathered.at[source(k), place(i)]
+        return remote(spot, spot, rsend.at[i, k], rrecv.at[i, k], {"tp": partner})
+
+    def push(i):
+        for k in range(1, chips):
+            forward(i, k).start()
+        relay(i, 0).start()
+
+    def stage(first):
+        def step(i):
+            finish(place(first + i))
+
+            @pl.when(i > 0)
+            def _():
+                push(first + i - 1)
+
+        each(half, step)
+        push(first + half - 1)
+
+    loads[-2].wait()
+    with jax.named_scope('fin1'):
+        stage(0)
     for c in range(chunks):
         for d in range(2):
-            answered(d, c).wait_recv()
-    each(half, lambda u: finish((1 - b) * half + u))
+            with jax.named_scope('answerw'):
+                answer(d, c, 1 - b).wait_recv()
+    with jax.named_scope('fin2'):
+        stage(half)
+
+    def multiply(src, h, start=False):
+        base = place(h * half)
+        left = jnp.concatenate([gathered[src, base + t] for t in range(half)], axis=1)
+        depth = half * LANES
+        right = matrix[pl.ds(pl.multiple_of((src * tiles + base) * LANES, LANES), depth), :]
+        value = jnp.dot(left, right, preferred_element_type=f32)
+        product[...] = value if start else product[...] + value
+
+    loads[-1].wait()
+    with jax.named_scope('mm0'):
+        multiply(j, 0, True)
+        multiply(j, 1)
+    for h in range(2):
+        with jax.named_scope('gatherw'):
+            for i in range(h * half, (h + 1) * half):
+                for k in range(1, chips):
+                    forward(i, k).wait_recv()
+                    relay(i, k).start()
+        for i in range(h * half, (h + 1) * half):
+            relay(i, 0).wait_recv()
+        multiply(partner, h)
+        for k in range(1, chips):
+            multiply(source(k), h)
+    for h in range(2):
+        for k in range(1, chips):
+            with jax.named_scope('relayw'):
+                for i in range(h * half, (h + 1) * half):
+                    relay(i, k).wait_recv()
+            multiply(source(k) + 1 - 2 * core, h)
+    rows = tokens // tp
+    width = product.shape[1]
+
+    def hand(d):
+        peer = lax.rem(j + d, tp)
+        return remote(mine.at[peer], theirs.at[j], psend.at[d], precv.at[d], {"tp": peer})
+
+    for d in list(range(1, tp)) + [0]:
+        peer = lax.rem(j + d, tp)
+        block = product[pl.ds(pl.multiple_of(peer * rows, rows), rows), :].astype(mine.dtype)
+        if d == 0:
+            out[:, pl.ds(pl.multiple_of(j * width, LANES), width)] = block
+        else:
+            mine[peer] = block
+    for d in range(1, tp):
+        hand(d).start()
+    for d in range(1, tp):
+        with jax.named_scope('handw'):
+            hand(d).wait_recv()
+        src = lax.rem(j + tp - d, tp)
+        out[:, pl.ds(pl.multiple_of(src * width, LANES), width)] = theirs[src]
+    for i in range(tiles):
+        for k in range(chips):
+            relay(i, k).wait_send()
+            if k > 0:
+                forward(i, k).wait_send()
+    for d in range(1, tp):
+        hand(d).wait_send()
 
     for way in range(2):
 
@@ -1015,8 +1168,8 @@
     for c in range(chunks):
         for d in range(2):
             ends = a == planes - 1 if d == 0 else a == 0
-            cross(d, c)[0].wait_send()
-            answer(d, c).wait_send()
+            cross(d, c).wait_send()
+            answer(d, c, b).wait_send()
 
             @pl.when(jnp.logical_not(ends))
             def _():
@@ -1024,10 +1177,11 @@
 
 
 def run_mixer(
-    value, key, query, gate, raw, rate, extra, vfilter, kfilter, qfilter, gain, number
+    value, key, query, gate, raw, rate, extra, vfilter, kfilter, qfilter, gain, matrix, number
 ):
-    n = lax.axis_size("sp")
+    n, tp = lax.axis_size("sp"), lax.axis_size("tp")
     tokens, wide = value.shape
+    rows, width = tokens // tp, matrix.shape[1]
     narrow = key.shape[1]
     groups, tiles = narrow // STATE, wide // LANES
     half = tiles // 2
@@ -1037,12 +1191,18 @@
     state = pltpu.VMEM((2, half, STATE, LANES), kind)
     full = pltpu.VMEM((2, tiles, STATE, LANES), kind)
     sems = dma(2, half // span)
+    operands = [
+        value, key, query, gate, raw.swapaxes(1, 2), rate, extra.T,
+        vfilter, kfilter, qfilter, gain.reshape(1, -1), matrix,
+    ]
+    pairs = dma(tiles, tp // 2)
     return pl.pallas_call(
         functools.partial(mixer_kernel, n, span),
-        out_shape=jax.ShapeDtypeStruct((tokens, wide), kind),
-        in_specs=vmem(11),
+        out_shape=jax.ShapeDtypeStruct((rows, tp * width), kind),
+        in_specs=[pl.BlockSpec(memory_space=pltpu.HBM)] * len(operands),
         out_specs=vmem(1)[0],
         scratch_shapes=[
+            *[pltpu.VMEM(x.shape, x.dtype) for x in operands],
             pltpu.VMEM((2, edge, wide), kind),
             pltpu.VMEM((2, edge, narrow), kind),
             pltpu.VMEM((2, edge, narrow), kind),
@@ -1051,18 +1211,23 @@
             pltpu.VMEM((tokens, narrow), kind),
             pltpu.VMEM((tokens, narrow), kind),
             pltpu.VMEM((groups, STATE, tokens), kind),
-            pltpu.VMEM((8, tokens, LANES), f32),
-            pltpu.VMEM((4, LANES, tokens), f32),
+            pltpu.VMEM((tokens, LANES), f32),
+            pltpu.VMEM((LANES, tokens), f32),
             pltpu.VMEM((2, 2, 8, LANES), f32),
             pltpu.VMEM((tokens, wide), f32),
             pltpu.VMEM((2, tokens, tokens), kind),
-            full, state, state, state, state, state, full,
-            dma(3, 2), dma(3, 2), dma(1), dma(1), sems, sems, sems, sems, sems, sems,
+            full, state, state, state, state, full,
+            pltpu.VMEM((tp, tiles, tokens, LANES), kind),
+            pltpu.VMEM((tokens, width), f32),
+            pltpu.VMEM((tp, rows, width), kind),
+            pltpu.VMEM((tp, rows, width), kind),
+            dma(3, 2), dma(3, 2), dma(1), dma(1), sems, sems, sems, sems, sems, sems, dma(len(operands)),
+            pairs, pairs, pairs, pairs, dma(tp), dma(tp),
         ],
         compiler_params=pltpu.CompilerParams(
-            collective_id=number, has_side_effects=True, vmem_limit_bytes=40 * 2**20
+            collective_id=number, has_side_effects=True
         ),
-    )(value, key, query, gate, raw, rate, extra, vfilter, kfilter, qfilter, gain.reshape(1, -1))
+    )(*operands)
 
 
 def slot_table(route_rows, experts, capacity):
@@ -1114,18 +1279,17 @@
         query_filter_weight,
         head_norm_gain,
     )
-    if value_projected.shape[1] % (2 * LANES) == 0 and lax.axis_size("sp") % 2 == 0:
-        heads_out = run_mixer(*operands, 2)
+    if value_projected.shape[1] % (2 * LANES) == 0 and 8 * step_projected_raw.shape[2] <= LANES and lax.axis_size("sp") % 2 == 0:
+        mixer_out = run_mixer(*operands, mixer_output_matrix, 2)
     else:
-        heads_out = mix_tokens(*operands)
-    projected = jnp.dot(
-        gather_columns(heads_out, 4),
-        mixer_output_matrix,
-        preferred_element_type=jnp.float32,
-    ).astype(jnp.bfloat16)
-    tp = lax.axis_size("tp")
-    (columns,) = exchange([projected.reshape(tp, -1, projected.shape[1])], "tp", 5)
-    mixer_out = columns.swapaxes(0, 1).reshape(columns.shape[1], -1)
+        projected = jnp.dot(
+            gather_columns(mix_tokens(*operands), 4),
+            mixer_output_matrix,
+            preferred_element_type=jnp.float32,
+        ).astype(jnp.bfloat16)
+        tp = lax.axis_size("tp")
+        (columns,) = exchange([projected.reshape(tp, -1, projected.shape[1])], "tp", 5)
+        mixer_out = columns.swapaxes(0, 1).reshape(columns.shape[1], -1)
     middle = (residual_layer_input.astype(jnp.float32) + mixer_out.astype(jnp.float32)).astype(
         jnp.bfloat16
     )

time: 187 us -> 133 us (0.71); the launches traced: 184 us -> 132 us
  Pallas kernels: 161 us -> 123 us
  local copies, waits for them, and re-layouts: 11.2 us -> 1.25 us
  matrix products: 8.89 us -> 5.07 us
    pallas_call x2 -> x0, Pallas kernels: 24.6 us -> none  [the longest x1 17.9 us: gather_columns(): pl.pallas_call(functools.partial(gather_kernel, tp, pieces), out_shape=ja...]
    pallas_call x1, Pallas kernels: 64.8 us -> 49.5 us  [run_mixer(): pl.pallas_call(functools.partial(mixer_kernel, n, span), out_shape=jax.Sh...]
    unnamed x28 -> x8, local copies, waits for them, and re-layouts: 9.92 us -> 0.01 us
    dot_general x1 -> x0, matrix products: 4.81 us -> none  [shards(): jnp.dot(gather_columns(heads_out, 4), mixer_output_matrix, preferred_elem...]
    pallas_call x1, Pallas kernels: 71.9 us -> 73.9 us  [run_experts(): pl.pallas_call(functools.partial(expert_kernel, sp, tp), out_shape=jax.Sh...]
where the time goes in v3:
time: 133 us; the launch traced here: 132 us
  Pallas kernels  123 us (92%)
  matrix products  5.07 us (4%)
  other arithmetic  2.53 us (2%)
    pallas_call x1, Pallas kernels, run_experts(): pl.pallas_call(functools.partial(expert_kernel, sp, tp), out_shape=jax.Sh...  73.9 us
    pallas_call x1, Pallas kernels, run_mixer(): pl.pallas_call(functools.partial(mixer_kernel, n, span), out_shape=jax.Sh...  49.5 us

profile of v3, /device:TPU:0, one launch (start us, length us, event | category | flops | bytes accessed | tf_op | source)
XLA Modules:
  0.0 132.3 jit_solution(7033628738728629937)
XLA Ops:
  0.0 0.0 copy-start.1
  0.0 0.0 copy-start.2
  0.0 0.8 constant_dynamic-slice_fusion
  0.8 0.1 copy.27
  0.9 0.1 eq.26
  1.0 0.1 fusion.7
  1.1 0.2 reduce_window_sum.11
  1.3 0.2 select_reduce_fusion.1
  1.5 0.1 reduce_sum.39
  1.6 0.1 copy.28
  1.7 0.8 multiply_add_fusion
  2.5 0.1 convert_reduce_fusion
  2.6 49.5 %shard_map.181 = bf16[64,2048]{1,0:T(8,128)(2,1)} custom-call(bf16[256,1024]{1,0:T(8,128)(2,1)} %far_value.1, bf16[256,512]{1,0:T(8,128)(2,1)} %far_key.1, bf16[256,512]{1,0:T(8,128)(2,1)} %far_query.1, bf16[256,1024]{1,0:T(8,128)(2,1)} %far_gate.1, bf16[2,16,256]{2,1,0:T(8,128)(2,1)} %bitcast.10, f32[2,16]{1,0:T(2,128)} %far_rate.1, f32[16,256]{1,0:T(8,128)} %bitcast.11, ...), custom_call_target="tpu_custom_call" | custom-call | tf_op jit(solution)/shard_map/pallas_call | solution.py:1199
  52.1 0.0 copy-done.1
  52.1 1.1 fusion.1
  53.3 0.0 copy-done.2
  53.3 2.5 %convolution_convert_fusion = bf16[256,2048]{1,0:T(8,128)(2,1)} fusion(f32[2048]{0:T(1024)S(1)} %copy-done.2, f32[64]{0:T(128)S(1)} %add_rsqrt_fusion, bf16[256,64]{0,1:T(8,128)(2,1)S(1)} %convert_reduce_fusion, bf16[64,2048]{1,0:T(8,128)(2,1)} %shard_map.181, bf16[64,2048]{1,0:T(8,128)(2,1)S(1)} %copy-done.1), kind=kOutput, calls=%fused_computation | convolution fusion | flops 68681728 | bytes 1614080 | tf_op jit(solution)/shard_map/dot_general | solution.py:1245
  55.7 0.0 copy-start.3
  55.7 0.0 copy-start
  55.7 73.9 %shard_map.182 = bf16[8,32,2048]{2,1,0:T(8,128)(2,1)} custom-call(bf16[8,32,2048]{2,1,0:T(8,128)(2,1)} %bitcast.9, bf16[1,2048,1024]{2,1,0:T(8,128)(2,1)} %wgate.1, bf16[1,2048,1024]{2,1,0:T(8,128)(2,1)} %wup.1, bf16[1,1024,2048]{2,1,0:T(8,128)(2,1)} %wdown.1), custom_call_target="tpu_custom_call" | custom-call | tf_op jit(solution)/shard_map/pallas_call | solution.py:585
  129.6 0.0 copy-done.3
  129.6 0.1 select_reduce_fusion
  129.7 0.0 copy-done
  129.7 2.6 %fusion = bf16[64,2048]{1,0:T(8,128)(2,1)} fusion(f32[64,256]{1,0:T(8,128)S(1)} %select_reduce_fusion, bf16[256,2048]{1,0:T(8,128)(2,1)} %bitcast.8, bf16[64,2048]{1,0:T(8,128)(2,1)S(1)} %copy-done, bf16[64,2048]{1,0:T(8,128)(2,1)S(1)} %copy-done.1), kind=kOutput, calls=%fused_computation.2 | convolution fusion | flops 403570688 | bytes 1900544 | tf_op jit(solution)/shard_map/dot_general | solution.py:1331
  (1 shorter events, 0.0 us)
Async XLA Ops:
  0.0 52.1 %copy-start.1 = (bf16[64,2048]{1,0:T(8,128)(2,1)S(1)}, bf16[64,2048]{1,0:T(8,128)(2,1)}, u32[]{:S(2)}) copy-start(bf16[64,2048]{1,0:T(8,128)(2,1)} %param.19) | copy-start | bytes 786436
  0.0 53.3 %copy-start.2 = (f32[2048]{0:T(1024)S(1)}, f32[2048]{0:T(1024)}, u32[]{:S(2)}) copy-start(f32[2048]{0:T(1024)} %param.32) | copy-start | bytes 24580
  55.7 73.9 %copy-start.3 = (f32[64,2]{0,1:T(2,128)S(1)}, f32[64,2]{0,1:T(2,128)}, u32[]{:S(2)}) copy-start(f32[64,2]{0,1:T(2,128)} %param.34) | copy-start | bytes 1540
  55.7 74.0 %copy-start = (bf16[64,2048]{1,0:T(8,128)(2,1)S(1)}, bf16[64,2048]{1,0:T(8,128)(2,1)}, u32[]{:S(2)}) copy-start(bf16[64,2048]{1,0:T(8,128)(2,1)} %shard_map.181) | copy-start | bytes 786436
